TPU v7x, 1024 devices: a whole 4x4x32 slice. The times are simulated.
1024 devices in a mesh: rep: 4 (over z_hi), fs: 32 (over z_lo, y), tp: 8 (over x, core).
Axes of the slice: x: 4, y: 4, z: 32 (z_hi: 4, z_lo: 8; z = z_hi * 8 + z_lo), core: 2. Of those that a mesh axis runs over, the one named last changes fastest.
Arguments:
- tokens: bfloat16 [128, 768, 2048], P(('rep', 'fs')), may hold values from -6 to 6
- norm_gain: float32 [2048], replicated, may hold values from 0.1 to 1.9
- outer_weight: bfloat16 [2048, 2048], P('fs', 'tp'), may hold values from -0.125 to 0.125
- inner_weight: bfloat16 [2048, 2048], P('fs', 'tp'), may hold values from -0.125 to 0.125
- value_weight: bfloat16 [2048, 2048], P('fs', 'tp'), may hold values from -0.125 to 0.125
- conv_taps: float32 [3, 2048], replicated, may hold values from -3.5 to 3.5
- out_weight: bfloat16 [2048, 2048], P('fs', 'tp'), may hold values from -0.125 to 0.125
Outputs:
- mixed: bfloat16 [128, 768, 2048], P(('rep', 'fs'), None, 'tp')
All inputs are finite; a program needn't handle non-finite values.
Results may differ from a plain program's by a relative error of at most 0.014.
Values may be sent and summed in bfloat16 or wider, within the bound.
No kernel may reach another device: no remote copies, remote signals or barrier semaphores. Data moves between devices by JAX's collectives and lax.ppermute only.
A program may use at most 32 MiB of HBM per device.

v0:
```python
import jax
import jax.numpy as jnp
from jax import lax
from jax.sharding import PartitionSpec as P


def laid_out(tiles, dim):
    tiles = jnp.moveaxis(tiles, 0, dim)
    lengths = tiles.shape
    return tiles.reshape(*lengths[:dim], lengths[dim] * lengths[dim + 1], *lengths[dim + 2 :])


def from_everyone(x, axis):
    peers = lax.axis_size(axis)
    return lax.all_to_all(jnp.broadcast_to(x[None], (peers, *x.shape)), axis, 0, 0, tiled=True)


def gather_directly(x, axis, dim):
    return laid_out(from_everyone(x, axis), dim)


def local(tokens, norm_gain, outer_weight, inner_weight, value_weight, conv_taps, out_weight):
    seq_len = tokens.shape[1]
    width = tokens.shape[2]
    xf = tokens.reshape(seq_len, width).astype(jnp.float32)
    scale = lax.rsqrt(jnp.mean(xf * xf, axis=-1, keepdims=True) + 1e-06)
    normed = (xf * scale * norm_gain).astype(jnp.bfloat16)
    columns = outer_weight.shape[1]

    def add_piece(piece):
        return jnp.dot(normed, piece, preferred_element_type=jnp.float32)

    outer = add_piece(gather_directly(outer_weight, "fs", 0))
    inner = add_piece(gather_directly(inner_weight, "fs", 0))
    value = add_piece(gather_directly(value_weight, "fs", 0))
    outer = outer.astype(jnp.bfloat16)
    inner = inner.astype(jnp.bfloat16)
    value = value.astype(jnp.bfloat16)
    product = inner.astype(jnp.float32) * value.astype(jnp.float32)
    offset = lax.axis_index("tp") * columns
    taps = lax.dynamic_slice_in_dim(conv_taps, offset, columns, 1)
    count = conv_taps.shape[0]
    padded = jnp.pad(product, ((count - 1, 0), (0, 0)))
    convolved = jnp.zeros((seq_len, columns), jnp.float32)
    for k in range(count):
        convolved = convolved + taps[k] * padded[k : k + seq_len, :]
    gated = (outer.astype(jnp.float32) * convolved).astype(jnp.bfloat16)
    everything = lax.all_gather(gated, "tp", axis=1, tiled=True)
    result = jnp.dot(
        everything, gather_directly(out_weight, "fs", 0), preferred_element_type=jnp.float32
    )
    return result.astype(jnp.bfloat16).reshape(1, seq_len, columns)


def solution(mesh):
    in_specs = (
        P(("rep", "fs"), None, None),
        P(),
        P("fs", "tp"),
        P("fs", "tp"),
        P("fs", "tp"),
        P(),
        P("fs", "tp"),
    )
    out_specs = P(("rep", "fs"), None, "tp")
    return jax.shard_map(local, mesh=mesh, in_specs=in_specs, out_specs=out_specs, check_vma=False)
```

profile of v0, /device:TPU:1, one launch (start us, length us, event | category | flops | bytes accessed | tf_op | source)
XLA Modules:
  0.0 267.6 jit_solution(2366755462462543095)
XLA Ops:
  6.5 0.9 broadcast_in_dim.8
  7.4 65.8 %all_to_all.20 = bf16[32,64,256]{2,1,0:T(8,128)(2,1)} all-to-all(bf16[32,64,256]{2,1,0:T(8,128)(2,1)S(1)} %broadcast_in_dim.8), channel_id=1, replica_groups=mesh['rep'=4,'fs'=32,'tp'=8] {'fs'}, dimensions={0} | all-to-all | bytes 2097152 | tf_op jit(solution)/shard_map/all_to_all | solution.py:15
  73.2 0.0 copy-done.4
  73.2 0.1 broadcast_in_dim.9
  73.3 57.8 %all_to_all.21 = bf16[32,64,256]{2,1,0:T(8,128)(2,1)} all-to-all(bf16[32,64,256]{2,1,0:T(8,128)(2,1)S(1)} %broadcast_in_dim.9), channel_id=1, replica_groups=mesh['rep'=4,'fs'=32,'tp'=8] {'fs'}, dimensions={0} | all-to-all | bytes 2097152 | tf_op jit(solution)/shard_map/all_to_all | solution.py:15
  131.1 0.0 copy-done.5
  131.1 0.1 broadcast_in_dim.10
  131.2 58.0 %all_to_all.22 = bf16[32,64,256]{2,1,0:T(8,128)(2,1)} all-to-all(bf16[32,64,256]{2,1,0:T(8,128)(2,1)S(1)} %broadcast_in_dim.10), channel_id=1, replica_groups=mesh['rep'=4,'fs'=32,'tp'=8] {'fs'}, dimensions={0} | all-to-all | bytes 2097152 | tf_op jit(solution)/shard_map/all_to_all | solution.py:15
  189.2 1.1 broadcast_in_dim.11
  190.3 8.2 %all-to-all-start.3 = ((bf16[32,64,256]{2,1,0:T(8,128)(2,1)}), bf16[32,64,256]{2,1,0:T(8,128)(2,1)}, u32[]{:S(2)}, u32[]{:S(2)}) async-start(bf16[32,64,256]{2,1,0:T(8,128)(2,1)} %broadcast_in_dim.11), calls=%async_computation.3 | async-start | bytes 2097152 | tf_op jit(solution)/shard_map/all_to_all | solution.py:15
  198.5 0.0 all-gather.2.cloned.1.call-start
  198.5 0.0 copy-start.2
  198.5 0.9 constant_dynamic-slice_fusion
  199.4 0.0 copy-done
  199.4 0.7 fusion
  200.1 1.0 fusion.6
  201.2 0.2 copy-done.3
  201.4 1.1 fusion.5
  202.4 0.2 copy-done.1
  202.6 1.9 fusion.9
  204.5 0.0 all-gather.2.cloned.1.call-update
  204.6 43.7 %all-to-all-done.3 = bf16[32,64,256]{2,1,0:T(8,128)(2,1)} async-done(((bf16[32,64,256]{2,1,0:T(8,128)(2,1)}), bf16[32,64,256]{2,1,0:T(8,128)(2,1)}, u32[]{:S(2)}, u32[]{:S(2)}) %all-to-all-start.3) | async-done | bytes 1048608 | tf_op jit(solution)/shard_map/all_to_all | solution.py:15
  248.2 8.6 %all-gather.2.cloned.1.call-done = bf16[768,2048]{1,0:T(8,128)(2,1)} async-done(((bf16[768,256]{1,0:T(8,128)(2,1)}), bf16[768,2048]{1,0:T(8,128)(2,1)}) %all-gather.2.cloned.1.call-update) | async-done | bytes 3145744 | tf_op jit(solution)/shard_map/all_gather | solution.py:48
  256.9 3.9 %fusion.10 = bf16[1,768,256]{2,1,0:T(8,128)(2,1)} fusion(bf16[768,2048]{1,0:T(8,128)(2,1)} %all-gather.2.cloned.1.call-done, bf16[2048,256]{1,0:T(8,128)(2,1)} %bitcast.7), kind=kOutput, calls=%fused_computation.16 | convolution fusion | flops 805502976 | bytes 4587520 | tf_op jit(solution)/shard_map/dot_general | solution.py:49
  (11 shorter events, 0.0 us)
Async XLA Ops:
  6.5 66.6 %copy-start.4 = (bf16[64,256]{1,0:T(8,128)(2,1)S(1)}, bf16[64,256]{1,0:T(8,128)(2,1)}, u32[]{:S(2)}) copy-start(bf16[64,256]{1,0:T(8,128)(2,1)} %param.10) | copy-start | bytes 98308
  6.5 124.5 %copy-start.5 = (bf16[64,256]{1,0:T(8,128)(2,1)S(1)}, bf16[64,256]{1,0:T(8,128)(2,1)}, u32[]{:S(2)}) copy-start(bf16[64,256]{1,0:T(8,128)(2,1)} %param.11) | copy-start | bytes 98308
  73.2 116.0 %copy-start.6 = (bf16[64,256]{1,0:T(8,128)(2,1)S(1)}, bf16[64,256]{1,0:T(8,128)(2,1)}, u32[]{:S(2)}) copy-start(bf16[64,256]{1,0:T(8,128)(2,1)} %param.13) | copy-start | bytes 98308
  131.1 68.3 %copy-start = (bf16[1,768,2048]{2,1,0:T(8,128)(2,1)S(1)}, bf16[1,768,2048]{2,1,0:T(8,128)(2,1)}, u32[]{:S(2)}) copy-start(bf16[1,768,2048]{2,1,0:T(8,128)(2,1)} %param.7) | copy-start | bytes 9437188
  189.2 10.9 %copy-start.7 = (f32[2048]{0:T(1024)S(1)}, f32[2048]{0:T(1024)}, u32[]{:S(2)}) copy-start(f32[2048]{0:T(1024)} %param.8) | copy-start | bytes 24580
  190.3 57.9 %all-to-all-start.3 = ((bf16[32,64,256]{2,1,0:T(8,128)(2,1)}), bf16[32,64,256]{2,1,0:T(8,128)(2,1)}, u32[]{:S(2)}, u32[]{:S(2)}) async-start(bf16[32,64,256]{2,1,0:T(8,128)(2,1)} %broadcast_in_dim.11), calls=%async_computation.3 | async-start | bytes 2097152 | tf_op jit(solution)/shard_map/all_to_all | solution.py:15
  198.5 58.4 %all-gather.2.cloned.1.call-start = ((), (), s32[]{:S(2)}) async-start(), calls=%async_computation.4 | async-start | bytes 3538944 | tf_op jit(solution)/shard_map/all_gather | solution.py:48
  198.5 1.6 copy-start.2
  200.1 1.2 copy-start.3
  201.4 1.2 copy-start.1
Sparse Core Ops, SparseCore 0:
  204.7 52.1 all-gather.1
where the time goes:
time: 268 us
  blocking collectives  182 us (68%)
  waiting for transfers between devices  52.3 us (20%)
  between operations  13.5 us (5%)
  starting transfers between devices  8.22 us (3%)
  matrix products  7.94 us (3%)
  local copies, waits for them, and re-layouts  3.41 us (1%)
    all_to_all x3, blocking collectives, from_everyone(): lax.all_to_all(jnp.broadcast_to(x[None], (peers, *x.shape)), axis, 0, 0,...  182 us
    all_to_all x1, waiting for transfers between devices, from_everyone(): lax.all_to_all(jnp.broadcast_to(x[None], (peers, *x.shape)), axis, 0, 0,...  43.7 us
    all_gather x1, waiting for transfers between devices, local(): everything = lax.all_gather(gated, 'tp', axis=1, tiled=True)  8.65 us
    all_to_all x1, starting transfers between devices, from_everyone(): lax.all_to_all(jnp.broadcast_to(x[None], (peers, *x.shape)), axis, 0, 0,...  8.18 us
  transfers between devices with their start and end apart: 2, of which 2 were waited for; matrix products, arithmetic and copies ran while one was open for 2% of the time, Pallas kernels for 0%

commit v1 on v0

v1 whole, which is shorter than its diff:
```python
import jax
import jax.numpy as jnp
from jax import lax
from jax.experimental import pallas as pl
from jax.experimental.pallas import tpu as pltpu
from jax.sharding import Mesh
from jax.sharding import PartitionSpec as P


LINE = ("rep", "zh", "zl")


def ring(size, step):
    return [(i, (i + step) % size) for i in range(size)]


def size_of(axis):
    names = (axis,) if isinstance(axis, str) else axis
    size = 1
    for name in names:
        size *= lax.axis_size(name)
    return size


def shift(x, axis, step):
    return lax.ppermute(x, axis, ring(size_of(axis), step))


def mirror(x):
    size = size_of(LINE)
    return lax.ppermute(x, LINE, [(i, (i + (-1, -3, 3, 1)[i % 4]) % size) for i in range(size)])


def copies_of(x, axis):
    return jnp.broadcast_to(x[None], (lax.axis_size(axis), *x.shape))


def exchange(copies, axis):
    return lax.all_to_all(copies, axis, 0, 0, tiled=True)


def pack_kernel(outer_ref, inner_ref, value_ref, out_ref):
    packed = jnp.concatenate([outer_ref[...], inner_ref[...], value_ref[...]], axis=1)
    for p in range(out_ref.shape[0]):
        out_ref[p] = packed


def norm_kernel(x_ref, gain_ref, out_ref):
    rows = 64
    gain = gain_ref[...]

    def step(i, _):
        at = pl.ds(pl.multiple_of(i * rows, rows), rows)
        x = x_ref[at, :].astype(jnp.float32)
        scale = lax.rsqrt(jnp.mean(x * x, axis=-1, keepdims=True) + 1e-06)
        out_ref[at, :] = (x * scale * gain).astype(jnp.bfloat16)
        return 0

    lax.fori_loop(0, x_ref.shape[0] // rows, step, 0)


ROWS = 256


def half_dot(normed_ref, weight_ref, group, r):
    depth = 256 * weight_ref.shape[1]
    at = pl.ds(pl.multiple_of(group * depth, depth), depth)
    weight = [weight_ref[:, b].reshape(256, weight_ref.shape[3]) for b in range(weight_ref.shape[1])]
    return jnp.dot(
        normed_ref[r : r + ROWS, at],
        jnp.concatenate(weight, axis=0),
        preferred_element_type=jnp.float32,
    )


def near_kernel(at_ref, normed_ref, weight_ref, total_ref):
    for r in range(0, normed_ref.shape[0], ROWS):
        total_ref[r : r + ROWS, :] = half_dot(normed_ref, weight_ref, at_ref[0], r)


def gate_kernel(at_ref, normed_ref, weight_ref, total_ref, taps_ref, out_ref, product):
    seq, columns = out_ref.shape
    product[0:8, :] = jnp.zeros((8, columns), jnp.float32)
    for r in range(0, seq, ROWS):
        parts = total_ref[r : r + ROWS, :] + half_dot(normed_ref, weight_ref, 1 - at_ref[0], r)
        parts = parts.astype(jnp.bfloat16).astype(jnp.float32)
        outer, inner, value = (parts[:, k * columns : (k + 1) * columns] for k in range(3))
        product[8 + r : 8 + r + ROWS, :] = inner * value
        convolved = taps_ref[0:1, :] * product[6 + r : 6 + r + ROWS, :]
        convolved = convolved + taps_ref[1:2, :] * product[7 + r : 7 + r + ROWS, :]
        convolved = convolved + taps_ref[2:3, :] * product[8 + r : 8 + r + ROWS, :]
        out_ref[r : r + ROWS, :] = (outer * convolved).astype(jnp.bfloat16)


def out_kernel(at_ref, *refs):
    gated, all_ref, out_ref = refs[:8], refs[8], refs[9]
    z, x, core = at_ref[1], at_ref[2], at_ref[3]
    seq, columns = out_ref.shape
    pieces = []
    for side in range(2):
        for step in (0, -1, 1, 2):
            tile = 2 * lax.rem(x + step + 4, 4) + lax.rem(core + side, 2)
            offset = lax.rem(tile - z + 12, 8)
            pieces.append(all_ref[:, offset].reshape(256, columns))
    weight = jnp.concatenate(pieces, axis=0)
    for r in range(0, seq, ROWS):
        left = jnp.concatenate([g[r : r + ROWS, :] for g in gated], axis=1)
        total = jnp.dot(left, weight, preferred_element_type=jnp.float32)
        out_ref[r : r + ROWS, :] = total.astype(jnp.bfloat16)


VMEM = pl.BlockSpec(memory_space=pltpu.VMEM)
SMEM = pl.BlockSpec(memory_space=pltpu.SMEM)


def call(kernel, shape, dtype, in_specs, flops, moved, scratch=(), limit=24):
    return pl.pallas_call(
        kernel,
        out_shape=jax.ShapeDtypeStruct(shape, dtype),
        in_specs=in_specs,
        out_specs=VMEM,
        scratch_shapes=list(scratch),
        cost_estimate=pl.CostEstimate(flops=flops, bytes_accessed=moved, transcendentals=0),
        compiler_params=pltpu.CompilerParams(vmem_limit_bytes=limit << 20),
    )


def gather_z(block):
    behind = shift(block, LINE, 1)
    ahead = shift(block, LINE, -1)
    near = jnp.stack([behind, block, ahead])
    low = shift(near, LINE, 3)
    high = shift(near[:2], LINE, -3)
    return jnp.concatenate([low, near, high])


def local(tokens, norm_gain, outer_weight, inner_weight, value_weight, conv_taps, out_weight):
    seq, width = tokens.shape[1:]
    depth, columns = outer_weight.shape
    bf16, f32 = jnp.bfloat16, jnp.float32
    half = lax.axis_index("zh")
    z = half * lax.axis_size("zl") + lax.axis_index("zl")
    x, core = lax.axis_index("x"), lax.axis_index("core")
    place = jnp.stack([half, z, x, core]).astype(jnp.int32)

    packed = call(pack_kernel, (4, depth, 3 * columns), bf16, [VMEM] * 3, 8 * depth * columns, 30 * depth * columns)
    group = exchange(packed(outer_weight, inner_weight, value_weight), "zl")
    other_group = mirror(group)
    near = exchange(copies_of(group, "y"), "y")

    norm = call(norm_kernel, (seq, width), bf16, [VMEM] * 2, 8 * seq * width, 4 * seq * width)
    normed = norm(tokens.reshape(seq, width), norm_gain.reshape(1, width))
    flops = 3 * seq * width * columns
    total = call(near_kernel, (seq, 3 * columns), f32, [SMEM] + [VMEM] * 2, flops, 8 * seq * width)(place, normed, near)
    far = exchange(copies_of(other_group, "y"), "y")

    out_rows = gather_z(out_weight)
    taps = lax.dynamic_slice_in_dim(conv_taps, (2 * x + core) * columns, columns, 1)
    gate = call(
        gate_kernel,
        (seq, columns),
        bf16,
        [SMEM] + [VMEM] * 4,
        flops,
        8 * seq * width,
        [pltpu.VMEM((8 + seq, columns), f32)],
    )
    gated = gate(place, normed, far, total, taps)

    own = [gated]
    for step in (1, -1, 2):
        own.append(shift(gated, "x", step))
    out_all = exchange(copies_of(out_rows, "y"), "y")
    other = [lax.ppermute(g, "core", [(0, 1), (1, 0)]) for g in own]
    project = call(out_kernel, (seq, columns), bf16, [SMEM] + [VMEM] * 9, 2 * seq * width * columns, 4 * seq * width)
    return project(place, *own, *other, out_all).reshape(1, seq, columns)


def solution(mesh):
    devices = mesh.devices.reshape(4, 2, 4, 4, 4, 2)
    fine = Mesh(devices, ("rep", "zh", "zl", "y", "x", "core"))
    fs, tp = ("zh", "zl", "y"), ("x", "core")
    in_specs = (
        P(("rep", *fs), None, None),
        P(),
        P(fs, tp),
        P(fs, tp),
        P(fs, tp),
        P(),
        P(fs, tp),
    )
    out_specs = P(("rep", *fs), None, tp)

    return jax.shard_map(local, mesh=fine, in_specs=in_specs, out_specs=out_specs, check_vma=False)
```

time: 268 us -> 131 us (0.49)
  blocking collectives: 182 us -> 14.1 us
  starting transfers between devices: 8.22 us -> 73.5 us
  waiting for transfers between devices: 52.3 us -> 17.4 us
  between operations: 13.5 us -> 0.3 us
  Pallas kernels: 0 us -> 11.5 us
  local copies, waits for them, and re-layouts: 3.41 us -> 13.1 us
  matrix products: 7.94 us -> 0 us
    all_to_all x3 -> x1, blocking collectives: 182 us -> 14.1 us  [exchange(): return lax.all_to_all(copies, axis, 0, 0, tiled=True)]
    ppermute x0 -> x12, starting transfers between devices: none -> 58.2 us  [the longest x7 23.5 us: shift(): return lax.ppermute(x, axis, ring(size_of(axis), step))]
    all_to_all x1 -> x3, waiting for transfers between devices: 43.7 us -> 5.92 us  [exchange(): return lax.all_to_all(copies, axis, 0, 0, tiled=True)]
    pallas_call x0 -> x5, Pallas kernels: none -> 11.5 us  [the longest x1 3.85 us: local(): gated = gate(place, normed, far, total, taps)]
    ppermute x0 -> x12, waiting for transfers between devices: none -> 11.5 us  [the longest x1 8.3 us: mirror(): lax.ppermute(x, LINE, [(i, (i + (-1, -3, 3, 1)[i % 4]) % size) for i in r...]
    all_gather x1 -> x0, waiting for transfers between devices: 8.65 us -> none  [local(): everything = lax.all_gather(gated, 'tp', axis=1, tiled=True)]
    dot_general x4 -> x0, matrix products: 7.94 us -> none  [the longest x3 4.04 us: add_piece(): return jnp.dot(normed, piece, preferred_element_type=jnp.float32)]
    all_to_all x1 -> x3, starting transfers between devices: 8.18 us -> 15.3 us  [exchange(): return lax.all_to_all(copies, axis, 0, 0, tiled=True)]
  transfers between devices with their start and end apart: 2 -> 15, of which waited for: 2 -> 5; matrix products, arithmetic and copies ran while one was open for 2% -> 3% of each run, Pallas kernels for 0% -> 4%
where the time goes in v1:
time: 131 us; the launch traced here: 130 us
  starting transfers between devices  73.5 us (56%)
  waiting for transfers between devices  17.4 us (13%)
  blocking collectives  14.1 us (11%)
  local copies, waits for them, and re-layouts  13.1 us (10%)
  Pallas kernels  11.5 us (9%)
    ppermute x7, starting transfers between devices, shift(): return lax.ppermute(x, axis, ring(size_of(axis), step))  23.5 us
    ppermute x4, starting transfers between devices, local(): other = [lax.ppermute(g, 'core', [(0, 1), (1, 0)]) for g in own]  18.4 us
    ppermute x1, starting transfers between devices, mirror(): lax.ppermute(x, LINE, [(i, (i + (-1, -3, 3, 1)[i % 4]) % size) for i in r...  16.2 us
    all_to_all x3, starting transfers between devices, exchange(): return lax.all_to_all(copies, axis, 0, 0, tiled=True)  15.3 us
    all_to_all x1, blocking collectives, exchange(): return lax.all_to_all(copies, axis, 0, 0, tiled=True)  14.1 us
    ppermute x1, waiting for transfers between devices, mirror(): lax.ppermute(x, LINE, [(i, (i + (-1, -3, 3, 1)[i % 4]) % size) for i in r...  8.3 us
    unnamed x22, local copies, waits for them, and re-layouts  7.31 us
    all_to_all x3, waiting for transfers between devices, exchange(): return lax.all_to_all(copies, axis, 0, 0, tiled=True)  5.92 us
  transfers between devices with their start and end apart: 15, of which 5 were waited for; matrix products, arithmetic and copies ran while one was open for 3% of the time, Pallas kernels for 4%

profile of v1, /device:TPU:1, one launch (start us, length us, event | category | flops | bytes accessed | tf_op | source)
XLA Modules:
  0.0 130.0 jit_solution(7109360609500544020)
XLA Ops:
  2.3 14.1 %all_to_all.20 = bf16[4,64,768]{2,1,0:T(8,128)(2,1)} all-to-all(bf16[4,64,768]{2,1,0:T(8,128)(2,1)S(1)} %shard_map.74), channel_id=1, replica_groups=mesh['rep'=4,'zh'=2,'zl'=4,'y'=4,'x'=4,'core'=2] {'zl'}, dimensions={0} | all-to-all | bytes 786432 | tf_op jit(solution)/shard_map/all_to_all | solution.py:39
  16.4 2.3 %broadcast_in_dim.7 = bf16[4,4,64,768]{3,2,1,0:T(8,128)(2,1)} broadcast(bf16[4,64,768]{2,1,0:T(8,128)(2,1)} %all_to_all.20), dimensions={1,2,3} | broadcast | bytes 1966080 | tf_op jit(solution)/shard_map/broadcast_in_dim | solution.py:35
  18.7 7.5 %all-to-all-start.2 = ((bf16[4,4,64,768]{3,2,1,0:T(8,128)(2,1)}), bf16[4,4,64,768]{3,2,1,0:T(8,128)(2,1)}, u32[]{:S(2)}, u32[]{:S(2)}) async-start(bf16[4,4,64,768]{3,2,1,0:T(8,128)(2,1)} %broadcast_in_dim.7), calls=%async_computation.2 | async-start | bytes 3145728 | tf_op jit(solution)/shard_map/all_to_all | solution.py:39
  26.1 16.2 %collective-permute-start = (bf16[4,64,768]{2,1,0:T(8,128)(2,1)}, bf16[4,64,768]{2,1,0:T(8,128)(2,1)}, u32[]{:S(2)}, u32[]{:S(2)}) collective-permute-start(bf16[4,64,768]{2,1,0:T(8,128)(2,1)} %all_to_all.20), channel_id=1, source_target_pairs={{0,992},{32,960},{64,160},{96,128},{128,96},{160,64},{192,288},{22... | collective-permute-start | bytes 1179656 | tf_op jit(solution)/shard_map/ppermute | solution.py:31
  42.4 1.9 %collective-permute-start.9 = (bf16[64,256]{1,0:T(8,128)(2,1)S(1)}, bf16[64,256]{1,0:T(8,128)(2,1)S(1)}, u32[]{:S(2)}, u32[]{:S(2)}) collective-permute-start(bf16[64,256]{1,0:T(8,128)(2,1)S(1)} %copy-done.8), channel_id=1, source_target_pairs={{0,992},{32,0},{64,32},{96,64},{128,96},{160,128},{192,160},{224,1... | collective-permute-start | bytes 98312 | tf_op jit(solution)/shard_map/ppermute | solution.py:26
  44.3 3.4 %collective-permute-start.8 = (bf16[64,256]{1,0:T(8,128)(2,1)S(1)}, bf16[64,256]{1,0:T(8,128)(2,1)S(1)}, u32[]{:S(2)}, u32[]{:S(2)}) collective-permute-start(bf16[64,256]{1,0:T(8,128)(2,1)S(1)} %copy-done.8), channel_id=1, source_target_pairs={{0,32},{32,64},{64,96},{96,128},{128,160},{160,192},{192,224},{224... | collective-permute-start | bytes 98312 | tf_op jit(solution)/shard_map/ppermute | solution.py:26
  49.7 2.0 %shard_map.73.normed_ref = bf16[768,2048]{1,0:T(8,128)(2,1)S(1)} custom-call(bf16[768,2048]{1,0:T(8,128)(2,1)S(1)} %bitcast.13, f32[1,2048]{1,0:T(1,128)S(1)} %bitcast.14), custom_call_target="tpu_custom_call" | custom-call | flops 12582912 | bytes 6291456 | tf_op jit(solution)/shard_map/pallas_call | solution.py:152
  51.7 8.3 %collective-permute-done = bf16[4,64,768]{2,1,0:T(8,128)(2,1)} collective-permute-done((bf16[4,64,768]{2,1,0:T(8,128)(2,1)}, bf16[4,64,768]{2,1,0:T(8,128)(2,1)}, u32[]{:S(2)}, u32[]{:S(2)}) %collective-permute-start) | collective-permute-done | bytes 393248 | tf_op jit(solution)/shard_map/ppermute | solution.py:31
  60.0 2.3 %broadcast_in_dim.6 = bf16[4,4,64,768]{3,2,1,0:T(8,128)(2,1)} broadcast(bf16[4,64,768]{2,1,0:T(8,128)(2,1)} %collective-permute-done), dimensions={1,2,3} | broadcast | bytes 1966080 | tf_op jit(solution)/shard_map/broadcast_in_dim | solution.py:35
  62.3 4.4 %all-to-all-start.1 = ((bf16[4,4,64,768]{3,2,1,0:T(8,128)(2,1)}), bf16[4,4,64,768]{3,2,1,0:T(8,128)(2,1)}, u32[]{:S(2)}, u32[]{:S(2)}) async-start(bf16[4,4,64,768]{3,2,1,0:T(8,128)(2,1)} %broadcast_in_dim.6), calls=%async_computation.1 | async-start | bytes 3145728 | tf_op jit(solution)/shard_map/all_to_all | solution.py:39
  66.7 1.9 %collective-permute-start.10 = (bf16[3,64,256]{2,1,0:T(8,128)(2,1)S(1)}, bf16[3,64,256]{2,1,0:T(8,128)(2,1)S(1)}, u32[]{:S(2)}, u32[]{:S(2)}) collective-permute-start(bf16[3,64,256]{2,1,0:T(8,128)(2,1)S(1)} %pad_maximum_fusion), channel_id=1, source_target_pairs={{0,96},{32,128},{64,160},{96,192},{128,224},{160,256},{192,288},{2... | collective-permute-start | bytes 294920 | tf_op jit(solution)/shard_map/ppermute | solution.py:26
  68.7 6.4 %collective-permute-start.11 = (bf16[2,64,256]{2,1,0:T(8,128)(2,1)S(1)}, bf16[2,64,256]{2,1,0:T(8,128)(2,1)S(1)}, u32[]{:S(2)}, u32[]{:S(2)}) collective-permute-start(bf16[2,64,256]{2,1,0:T(8,128)(2,1)S(1)} %pad_maximum_fusion.1), channel_id=1, source_target_pairs={{0,928},{32,960},{64,992},{96,0},{128,32},{160,64},{192,96},{224,1... | collective-permute-start | bytes 196616 | tf_op jit(solution)/shard_map/ppermute | solution.py:26
  76.5 2.8 %shard_map.75.total_ref = f32[768,768]{1,0:T(8,128)S(1)} custom-call(s32[4]{0:T(128)S(1)} %pad_add_fusion.at_ref, bf16[768,2048]{1,0:T(8,128)(2,1)S(1)} %shard_map.73.normed_ref, bf16[4,4,64,768]{3,2,1,0:T(8,128)(2,1)} %all-to-all-done.2.weight_ref), custom_call_target="tpu_custom_call" | custom-call | flops 1207959552 | bytes 12582912 | tf_op jit(solution)/shard_map/pallas_call | solution.py:154
  80.8 5.9 %all-to-all-done.1.weight_ref = bf16[4,4,64,768]{3,2,1,0:T(8,128)(2,1)} async-done(((bf16[4,4,64,768]{3,2,1,0:T(8,128)(2,1)}), bf16[4,4,64,768]{3,2,1,0:T(8,128)(2,1)}, u32[]{:S(2)}, u32[]{:S(2)}) %all-to-all-start.1) | async-done | bytes 1572896 | tf_op jit(solution)/shard_map/all_to_all | solution.py:39
  88.3 3.9 %shard_map.76.refs_0_ = bf16[768,256]{1,0:T(8,128)(2,1)} custom-call(s32[4]{0:T(128)S(1)} %pad_add_fusion.at_ref, bf16[768,2048]{1,0:T(8,128)(2,1)S(1)} %shard_map.73.normed_ref, bf16[4,4,64,768]{3,2,1,0:T(8,128)(2,1)} %all-to-all-done.1.weight_ref, f32[768,768]{1,0:T(8,128)S(1)} %copy-done.2, f32[3,256]{1,0:T(4,128)S(1)} %constant_dynamic-slice_fusion.taps_ref), custom_call_target="tpu_custom_call" | custom-call | flops 1207959552 | bytes 12582912 | tf_op jit(solution)/shard_map/pallas_call | solution.py:168
  92.2 3.1 %collective-permute-start.1 = (bf16[768,256]{1,0:T(8,128)(2,1)}, bf16[768,256]{1,0:T(8,128)(2,1)S(1)}, u32[]{:S(2)}, u32[]{:S(2)}) collective-permute-start(bf16[768,256]{1,0:T(8,128)(2,1)} %shard_map.76.refs_0_), channel_id=1, source_target_pairs={{0,2},{2,4},{4,6},{6,0},{1,3},{3,5},{5,7},{7,1},{8,10},{10,12},{12... | collective-permute-start | bytes 1179656 | tf_op jit(solution)/shard_map/ppermute | solution.py:26
  96.4 3.5 %all-to-all-start.3 = ((bf16[4,8,64,256]{3,2,1,0:T(8,128)(2,1)}), bf16[4,8,64,256]{3,2,1,0:T(8,128)(2,1)S(1)}, u32[]{:S(2)}, u32[]{:S(2)}) async-start(bf16[4,8,64,256]{3,2,1,0:T(8,128)(2,1)} %broadcast_in_dim.8), calls=%async_computation.3 | async-start | bytes 2097152 | tf_op jit(solution)/shard_map/all_to_all | solution.py:39
  100.0 3.4 %collective-permute-start.2 = (bf16[768,256]{1,0:T(8,128)(2,1)}, bf16[768,256]{1,0:T(8,128)(2,1)S(1)}, u32[]{:S(2)}, u32[]{:S(2)}) collective-permute-start(bf16[768,256]{1,0:T(8,128)(2,1)} %shard_map.76.refs_0_), channel_id=1, source_target_pairs={{0,6},{2,0},{4,2},{6,4},{1,7},{3,1},{5,3},{7,5},{8,14},{10,8},{12,... | collective-permute-start | bytes 1179656 | tf_op jit(solution)/shard_map/ppermute | solution.py:26
  103.4 3.4 %collective-permute-start.3 = (bf16[768,256]{1,0:T(8,128)(2,1)}, bf16[768,256]{1,0:T(8,128)(2,1)S(1)}, u32[]{:S(2)}, u32[]{:S(2)}) collective-permute-start(bf16[768,256]{1,0:T(8,128)(2,1)} %shard_map.76.refs_0_), channel_id=1, source_target_pairs={{0,4},{2,6},{4,0},{6,2},{1,5},{3,7},{5,1},{7,3},{8,12},{10,14},{12... | collective-permute-start | bytes 1179656 | tf_op jit(solution)/shard_map/ppermute | solution.py:26
  106.8 4.5 %collective-permute-start.4 = (bf16[768,256]{1,0:T(8,128)(2,1)}, bf16[768,256]{1,0:T(8,128)(2,1)S(1)}, u32[]{:S(2)}, u32[]{:S(2)}) collective-permute-start(bf16[768,256]{1,0:T(8,128)(2,1)} %shard_map.76.refs_0_), channel_id=1, source_target_pairs={{0,1},{1,0},{2,3},{3,2},{4,5},{5,4},{6,7},{7,6},{8,9},{9,8},{10,11... | collective-permute-start | bytes 1179656 | tf_op jit(solution)/shard_map/ppermute | solution.py:174
  111.3 1.9 %collective-permute-start.5 = (bf16[768,256]{1,0:T(8,128)(2,1)S(1)}, bf16[768,256]{1,0:T(8,128)(2,1)S(1)}, u32[]{:S(2)}, u32[]{:S(2)}) collective-permute-start(bf16[768,256]{1,0:T(8,128)(2,1)S(1)} %collective-permute-done.1.refs_1_), channel_id=1, source_target_pairs={{0,1},{1,0},{2,3},{3,2},{4,5},{5,4},{6,7},{7,6},{8,9},{9,8},{10,11... | collective-permute-start | bytes 1179656 | tf_op jit(solution)/shard_map/ppermute | solution.py:174
  113.2 10.1 %collective-permute-start.6 = (bf16[768,256]{1,0:T(8,128)(2,1)S(1)}, bf16[768,256]{1,0:T(8,128)(2,1)S(1)}, u32[]{:S(2)}, u32[]{:S(2)}) collective-permute-start(bf16[768,256]{1,0:T(8,128)(2,1)S(1)} %collective-permute-done.2.refs_2_), channel_id=1, source_target_pairs={{0,1},{1,0},{2,3},{3,2},{4,5},{5,4},{6,7},{7,6},{8,9},{9,8},{10,11... | collective-permute-start | bytes 1179656 | tf_op jit(solution)/shard_map/ppermute | solution.py:174
  123.3 1.9 %collective-permute-start.7 = (bf16[768,256]{1,0:T(8,128)(2,1)S(1)}, bf16[768,256]{1,0:T(8,128)(2,1)}, u32[]{:S(2)}, u32[]{:S(2)}) collective-permute-start(bf16[768,256]{1,0:T(8,128)(2,1)S(1)} %collective-permute-done.3.refs_3_), channel_id=1, source_target_pairs={{0,1},{1,0},{2,3},{3,2},{4,5},{5,4},{6,7},{7,6},{8,9},{9,8},{10,11... | collective-permute-start | bytes 1179656 | tf_op jit(solution)/shard_map/ppermute | solution.py:174
  127.1 2.9 %shard_map.77 = bf16[768,256]{1,0:T(8,128)(2,1)} custom-call(s32[4]{0:T(128)S(1)} %pad_add_fusion.at_ref, bf16[768,256]{1,0:T(8,128)(2,1)} %shard_map.76.refs_0_, bf16[768,256]{1,0:T(8,128)(2,1)S(1)} %collective-permute-done.1.refs_1_, bf16[768,256]{1,0:T(8,128)(2,1)S(1)} %collective-permute-done.2.refs_2_, ...), custom_call_target="tpu_custom_call" | custom-call | flops 805306368 | bytes 6291456 | tf_op jit(solution)/shard_map/pallas_call | solution.py:176
  (42 shorter events, 11.8 us)
Async XLA Ops:
  0.0 47.7 %copy-start = (f32[3,2048]{1,0:T(4,128)S(1)}, f32[3,2048]{1,0:T(4,128)}, u32[]{:S(2)}) copy-start(f32[3,2048]{1,0:T(4,128)} %param.12) | copy-start | bytes 73732
  0.0 0.8 copy-start.4
  0.8 0.8 copy-start.5
  1.5 0.8 copy-start.6
  18.7 23.7 %copy-start.8 = (bf16[64,256]{1,0:T(8,128)(2,1)S(1)}, bf16[64,256]{1,0:T(8,128)(2,1)}, u32[]{:S(2)}) copy-start(bf16[64,256]{1,0:T(8,128)(2,1)} %param.13) | copy-start | bytes 98308
  18.7 29.1 %copy-start.7 = (f32[2048]{0:T(1024)S(1)}, f32[2048]{0:T(1024)}, u32[]{:S(2)}) copy-start(f32[2048]{0:T(1024)} %param.8) | copy-start | bytes 24580
  18.7 41.3 %all-to-all-start.2 = ((bf16[4,4,64,768]{3,2,1,0:T(8,128)(2,1)}), bf16[4,4,64,768]{3,2,1,0:T(8,128)(2,1)}, u32[]{:S(2)}, u32[]{:S(2)}) async-start(bf16[4,4,64,768]{3,2,1,0:T(8,128)(2,1)} %broadcast_in_dim.7), calls=%async_computation.2 | async-start | bytes 3145728 | tf_op jit(solution)/shard_map/all_to_all | solution.py:39
  26.1 33.9 %collective-permute-start = (bf16[4,64,768]{2,1,0:T(8,128)(2,1)}, bf16[4,64,768]{2,1,0:T(8,128)(2,1)}, u32[]{:S(2)}, u32[]{:S(2)}) collective-permute-start(bf16[4,64,768]{2,1,0:T(8,128)(2,1)} %all_to_all.20), channel_id=1, source_target_pairs={{0,992},{32,960},{64,160},{96,128},{128,96},{160,64},{192,288},{22... | collective-permute-start | bytes 1179656 | tf_op jit(solution)/shard_map/ppermute | solution.py:31
  42.4 24.3 %collective-permute-start.9 = (bf16[64,256]{1,0:T(8,128)(2,1)S(1)}, bf16[64,256]{1,0:T(8,128)(2,1)S(1)}, u32[]{:S(2)}, u32[]{:S(2)}) collective-permute-start(bf16[64,256]{1,0:T(8,128)(2,1)S(1)} %copy-done.8), channel_id=1, source_target_pairs={{0,992},{32,0},{64,32},{96,64},{128,96},{160,128},{192,160},{224,1... | collective-permute-start | bytes 98312 | tf_op jit(solution)/shard_map/ppermute | solution.py:26
  44.3 22.4 %collective-permute-start.8 = (bf16[64,256]{1,0:T(8,128)(2,1)S(1)}, bf16[64,256]{1,0:T(8,128)(2,1)S(1)}, u32[]{:S(2)}, u32[]{:S(2)}) collective-permute-start(bf16[64,256]{1,0:T(8,128)(2,1)S(1)} %copy-done.8), channel_id=1, source_target_pairs={{0,32},{32,64},{64,96},{96,128},{128,160},{160,192},{192,224},{224... | collective-permute-start | bytes 98312 | tf_op jit(solution)/shard_map/ppermute | solution.py:26
  47.8 1.9 %copy-start.3 = (bf16[1,768,2048]{2,1,0:T(8,128)(2,1)S(1)}, bf16[1,768,2048]{2,1,0:T(8,128)(2,1)}, u32[]{:S(2)}) copy-start(bf16[1,768,2048]{2,1,0:T(8,128)(2,1)} %param.7) | copy-start | bytes 9437188
  62.3 24.3 %all-to-all-start.1 = ((bf16[4,4,64,768]{3,2,1,0:T(8,128)(2,1)}), bf16[4,4,64,768]{3,2,1,0:T(8,128)(2,1)}, u32[]{:S(2)}, u32[]{:S(2)}) async-start(bf16[4,4,64,768]{3,2,1,0:T(8,128)(2,1)} %broadcast_in_dim.6), calls=%async_computation.1 | async-start | bytes 3145728 | tf_op jit(solution)/shard_map/all_to_all | solution.py:39
  66.7 8.5 %collective-permute-start.10 = (bf16[3,64,256]{2,1,0:T(8,128)(2,1)S(1)}, bf16[3,64,256]{2,1,0:T(8,128)(2,1)S(1)}, u32[]{:S(2)}, u32[]{:S(2)}) collective-permute-start(bf16[3,64,256]{2,1,0:T(8,128)(2,1)S(1)} %pad_maximum_fusion), channel_id=1, source_target_pairs={{0,96},{32,128},{64,160},{96,192},{128,224},{160,256},{192,288},{2... | collective-permute-start | bytes 294920 | tf_op jit(solution)/shard_map/ppermute | solution.py:26
  68.7 7.8 %collective-permute-start.11 = (bf16[2,64,256]{2,1,0:T(8,128)(2,1)S(1)}, bf16[2,64,256]{2,1,0:T(8,128)(2,1)S(1)}, u32[]{:S(2)}, u32[]{:S(2)}) collective-permute-start(bf16[2,64,256]{2,1,0:T(8,128)(2,1)S(1)} %pad_maximum_fusion.1), channel_id=1, source_target_pairs={{0,928},{32,960},{64,992},{96,0},{128,32},{160,64},{192,96},{224,1... | collective-permute-start | bytes 196616 | tf_op jit(solution)/shard_map/ppermute | solution.py:26
  79.3 1.4 %copy-start.1 = (f32[768,768]{1,0:T(8,128)}, f32[768,768]{1,0:T(8,128)S(1)}, u32[]{:S(2)}) copy-start(f32[768,768]{1,0:T(8,128)S(1)} %shard_map.75.total_ref) | copy-start | bytes 7077892
  86.7 1.7 %copy-start.2 = (f32[768,768]{1,0:T(8,128)S(1)}, f32[768,768]{1,0:T(8,128)}, u32[]{:S(2)}) copy-start(f32[768,768]{1,0:T(8,128)} %copy-done.1) | copy-start | bytes 7077892
  92.2 19.1 %collective-permute-start.1 = (bf16[768,256]{1,0:T(8,128)(2,1)}, bf16[768,256]{1,0:T(8,128)(2,1)S(1)}, u32[]{:S(2)}, u32[]{:S(2)}) collective-permute-start(bf16[768,256]{1,0:T(8,128)(2,1)} %shard_map.76.refs_0_), channel_id=1, source_target_pairs={{0,2},{2,4},{4,6},{6,0},{1,3},{3,5},{5,7},{7,1},{8,10},{10,12},{12... | collective-permute-start | bytes 1179656 | tf_op jit(solution)/shard_map/ppermute | solution.py:26
  96.4 28.8 %all-to-all-start.3 = ((bf16[4,8,64,256]{3,2,1,0:T(8,128)(2,1)}), bf16[4,8,64,256]{3,2,1,0:T(8,128)(2,1)S(1)}, u32[]{:S(2)}, u32[]{:S(2)}) async-start(bf16[4,8,64,256]{3,2,1,0:T(8,128)(2,1)} %broadcast_in_dim.8), calls=%async_computation.3 | async-start | bytes 2097152 | tf_op jit(solution)/shard_map/all_to_all | solution.py:39
  100.0 13.3 %collective-permute-start.2 = (bf16[768,256]{1,0:T(8,128)(2,1)}, bf16[768,256]{1,0:T(8,128)(2,1)S(1)}, u32[]{:S(2)}, u32[]{:S(2)}) collective-permute-start(bf16[768,256]{1,0:T(8,128)(2,1)} %shard_map.76.refs_0_), channel_id=1, source_target_pairs={{0,6},{2,0},{4,2},{6,4},{1,7},{3,1},{5,3},{7,5},{8,14},{10,8},{12,... | collective-permute-start | bytes 1179656 | tf_op jit(solution)/shard_map/ppermute | solution.py:26
  103.4 20.0 %collective-permute-start.3 = (bf16[768,256]{1,0:T(8,128)(2,1)}, bf16[768,256]{1,0:T(8,128)(2,1)S(1)}, u32[]{:S(2)}, u32[]{:S(2)}) collective-permute-start(bf16[768,256]{1,0:T(8,128)(2,1)} %shard_map.76.refs_0_), channel_id=1, source_target_pairs={{0,4},{2,6},{4,0},{6,2},{1,5},{3,7},{5,1},{7,3},{8,12},{10,14},{12... | collective-permute-start | bytes 1179656 | tf_op jit(solution)/shard_map/ppermute | solution.py:26
  106.8 18.5 %collective-permute-start.4 = (bf16[768,256]{1,0:T(8,128)(2,1)}, bf16[768,256]{1,0:T(8,128)(2,1)S(1)}, u32[]{:S(2)}, u32[]{:S(2)}) collective-permute-start(bf16[768,256]{1,0:T(8,128)(2,1)} %shard_map.76.refs_0_), channel_id=1, source_target_pairs={{0,1},{1,0},{2,3},{3,2},{4,5},{5,4},{6,7},{7,6},{8,9},{9,8},{10,11... | collective-permute-start | bytes 1179656 | tf_op jit(solution)/shard_map/ppermute | solution.py:174
  111.3 14.0 %collective-permute-start.5 = (bf16[768,256]{1,0:T(8,128)(2,1)S(1)}, bf16[768,256]{1,0:T(8,128)(2,1)S(1)}, u32[]{:S(2)}, u32[]{:S(2)}) collective-permute-start(bf16[768,256]{1,0:T(8,128)(2,1)S(1)} %collective-permute-done.1.refs_1_), channel_id=1, source_target_pairs={{0,1},{1,0},{2,3},{3,2},{4,5},{5,4},{6,7},{7,6},{8,9},{9,8},{10,11... | collective-permute-start | bytes 1179656 | tf_op jit(solution)/shard_map/ppermute | solution.py:174
  113.2 12.1 %collective-permute-start.6 = (bf16[768,256]{1,0:T(8,128)(2,1)S(1)}, bf16[768,256]{1,0:T(8,128)(2,1)S(1)}, u32[]{:S(2)}, u32[]{:S(2)}) collective-permute-start(bf16[768,256]{1,0:T(8,128)(2,1)S(1)} %collective-permute-done.2.refs_2_), channel_id=1, source_target_pairs={{0,1},{1,0},{2,3},{3,2},{4,5},{5,4},{6,7},{7,6},{8,9},{9,8},{10,11... | collective-permute-start | bytes 1179656 | tf_op jit(solution)/shard_map/ppermute | solution.py:174
  123.3 3.7 %collective-permute-start.7 = (bf16[768,256]{1,0:T(8,128)(2,1)S(1)}, bf16[768,256]{1,0:T(8,128)(2,1)}, u32[]{:S(2)}, u32[]{:S(2)}) collective-permute-start(bf16[768,256]{1,0:T(8,128)(2,1)S(1)} %collective-permute-done.3.refs_3_), channel_id=1, source_target_pairs={{0,1},{1,0},{2,3},{3,2},{4,5},{5,4},{6,7},{7,6},{8,9},{9,8},{10,11... | collective-permute-start | bytes 1179656 | tf_op jit(solution)/shard_map/ppermute | solution.py:174

commit v2 on v1

v2 whole, which is shorter than its diff:
```python
import jax
import jax.numpy as jnp
from jax import lax
from jax.experimental import pallas as pl
from jax.experimental.pallas import tpu as pltpu
from jax.sharding import Mesh
from jax.sharding import PartitionSpec as P


LINE = ("rep", "zh", "zl")


def ring(size, step):
    return [(i, (i + step) % size) for i in range(size)]


def size_of(axis):
    names = (axis,) if isinstance(axis, str) else axis
    size = 1
    for name in names:
        size *= lax.axis_size(name)
    return size


def shift(x, axis, step):
    return lax.ppermute(x, axis, ring(size_of(axis), step))


def mirror(x):
    size = size_of(LINE)
    return lax.ppermute(x, LINE, [(i, (i + (-1, -3, 3, 1)[i % 4]) % size) for i in range(size)])


def exchange(copies, axis):
    return lax.all_to_all(copies, axis, 0, 0, tiled=True)


def pack_kernel(outer_ref, inner_ref, value_ref, out_ref, held, sems):
    copies = [
        pltpu.make_async_copy(ref, held.at[k], sems.at[k])
        for k, ref in enumerate((outer_ref, inner_ref, value_ref))
    ]
    for copy in copies:
        copy.start()
    columns = held.shape[2]
    for k, copy in enumerate(copies):
        copy.wait()
        for p in range(out_ref.shape[0]):
            out_ref[p, :, k * columns : (k + 1) * columns] = held[k]


def norm_kernel(x_ref, gain_ref, out_ref):
    rows = 64
    gain = gain_ref[...]

    def step(i, _):
        at = pl.ds(pl.multiple_of(i * rows, rows), rows)
        x = x_ref[at, :].astype(jnp.float32)
        scale = lax.rsqrt(jnp.mean(x * x, axis=-1, keepdims=True) + 1e-06)
        out_ref[at, :] = (x * scale * gain).astype(jnp.bfloat16)
        return 0

    lax.fori_loop(0, x_ref.shape[0] // rows, step, 0)


ROWS = 256
STEPS = (0, -1, 1, 2)


def place_rows(at_ref, pieces, weight):
    for piece, step in zip(pieces, STEPS):
        y = lax.rem(at_ref[4] + step + 4, 4)
        for b in range(piece.shape[0]):
            weight[pl.ds(pl.multiple_of(b * 256 + y * 64, 64), 64), :] = piece[b]


def half_dot(normed_ref, weight, group, r):
    depth = weight.shape[0]
    at = pl.ds(pl.multiple_of(group * depth, depth), depth)
    return jnp.dot(normed_ref[r : r + ROWS, at], weight[...], preferred_element_type=jnp.float32)


def near_kernel(at_ref, normed_ref, *refs):
    pieces, total_ref, weight = refs[:4], refs[4], refs[5]
    place_rows(at_ref, pieces, weight)
    for r in range(0, normed_ref.shape[0], ROWS):
        total_ref[r : r + ROWS, :] = half_dot(normed_ref, weight, at_ref[0], r)


def gate_kernel(at_ref, normed_ref, *refs):
    pieces, total_ref, taps_ref, out_ref, weight, product = refs[:4], *refs[4:]
    place_rows(at_ref, pieces, weight)
    seq, columns = out_ref.shape
    product[0:8, :] = jnp.zeros((8, columns), jnp.float32)
    for r in range(0, seq, ROWS):
        parts = total_ref[r : r + ROWS, :] + half_dot(normed_ref, weight, 1 - at_ref[0], r)
        parts = parts.astype(jnp.bfloat16).astype(jnp.float32)
        outer, inner, value = (parts[:, k * columns : (k + 1) * columns] for k in range(3))
        product[8 + r : 8 + r + ROWS, :] = inner * value
        convolved = taps_ref[0:1, :] * product[6 + r : 6 + r + ROWS, :]
        convolved = convolved + taps_ref[1:2, :] * product[7 + r : 7 + r + ROWS, :]
        convolved = convolved + taps_ref[2:3, :] * product[8 + r : 8 + r + ROWS, :]
        out_ref[r : r + ROWS, :] = (outer * convolved).astype(jnp.bfloat16)


def out_kernel(at_ref, *refs):
    gated, pieces, out_ref, weight = refs[:8], refs[8:12], refs[12], refs[13]
    z, x, core, y = at_ref[1], at_ref[2], at_ref[3], at_ref[4]
    for side in range(2):
        for k, step in enumerate(STEPS):
            tile = 2 * lax.rem(x + step + 4, 4) + lax.rem(core + side, 2)
            offset = lax.rem(tile - z + 12, 8)
            for piece, other in zip(pieces, STEPS):
                at = (side * 4 + k) * 256 + lax.rem(y + other + 4, 4) * 64
                weight[pl.ds(pl.multiple_of(at, 64), 64), :] = piece[offset]
    for r in range(0, out_ref.shape[0], ROWS):
        left = jnp.concatenate([g[r : r + ROWS, :] for g in gated], axis=1)
        total = jnp.dot(left, weight[...], preferred_element_type=jnp.float32)
        out_ref[r : r + ROWS, :] = total.astype(jnp.bfloat16)


VMEM = pl.BlockSpec(memory_space=pltpu.VMEM)
ANY = pl.BlockSpec(memory_space=pl.ANY)
SMEM = pl.BlockSpec(memory_space=pltpu.SMEM)


def call(kernel, shape, dtype, in_specs, flops, moved, scratch=(), limit=24):
    return pl.pallas_call(
        kernel,
        out_shape=jax.ShapeDtypeStruct(shape, dtype),
        in_specs=in_specs,
        out_specs=VMEM,
        scratch_shapes=list(scratch),
        cost_estimate=pl.CostEstimate(flops=flops, bytes_accessed=moved, transcendentals=0),
        compiler_params=pltpu.CompilerParams(vmem_limit_bytes=limit << 20),
    )


def pieces_of(x, axis):
    pieces = [x]
    for step in (1, -1, 2):
        pieces.append(shift(x, axis, step))
    return pieces


def gather_z(block):
    behind = shift(block, LINE, 1)
    ahead = shift(block, LINE, -1)
    near = jnp.stack([behind, block, ahead])
    low = shift(near, LINE, 3)
    high = shift(near[:2], LINE, -3)
    return jnp.concatenate([low, near, high])


def local(tokens, norm_gain, outer_weight, inner_weight, value_weight, conv_taps, out_weight):
    seq, width = tokens.shape[1:]
    depth, columns = outer_weight.shape
    bf16, f32 = jnp.bfloat16, jnp.float32
    half = lax.axis_index("zh")
    z = half * lax.axis_size("zl") + lax.axis_index("zl")
    x, core = lax.axis_index("x"), lax.axis_index("core")
    place = jnp.stack([half, z, x, core, lax.axis_index("y")]).astype(jnp.int32)

    packed = call(
        pack_kernel,
        (4, depth, 3 * columns),
        bf16,
        [ANY] * 3,
        8 * depth * columns,
        30 * depth * columns,
        [pltpu.VMEM((3, depth, columns), bf16), pltpu.SemaphoreType.DMA((3,))],
        limit=60,
    )
    group = exchange(packed(outer_weight, inner_weight, value_weight), "zl")
    other_group = mirror(group)
    near = pieces_of(group, "y")

    norm = call(norm_kernel, (seq, width), bf16, [VMEM] * 2, 8 * seq * width, 4 * seq * width)
    normed = norm(tokens.reshape(seq, width), norm_gain.reshape(1, width))
    flops = 3 * seq * width * columns
    weight = pltpu.VMEM((width // 2, 3 * columns), bf16)
    start = call(
        near_kernel, (seq, 3 * columns), f32, [SMEM] + [VMEM] * 5, flops, 8 * seq * width, [weight]
    )
    total = start(place, normed, *near)
    far = pieces_of(other_group, "y")

    out_rows = gather_z(out_weight)
    taps = lax.dynamic_slice_in_dim(conv_taps, (2 * x + core) * columns, columns, 1)
    gate = call(
        gate_kernel,
        (seq, columns),
        bf16,
        [SMEM] + [VMEM] * 7,
        flops,
        8 * seq * width,
        [weight, pltpu.VMEM((8 + seq, columns), f32)],
    )
    rows = pieces_of(out_rows, "y")
    gated = gate(place, normed, *far, total, taps)

    own = pieces_of(gated, "x")
    other = []
    for g in own:
        other.append(lax.ppermute(g, "core", [(0, 1), (1, 0)]))
    project = call(
        out_kernel,
        (seq, columns),
        bf16,
        [SMEM] + [VMEM] * 12,
        2 * seq * width * columns,
        4 * seq * width,
        [pltpu.VMEM((width, columns), bf16)],
    )
    return project(place, *own, *other, *rows).reshape(1, seq, columns)


def solution(mesh):
    devices = mesh.devices.reshape(4, 2, 4, 4, 4, 2)
    fine = Mesh(devices, ("rep", "zh", "zl", "y", "x", "core"))
    fs, tp = ("zh", "zl", "y"), ("x", "core")
    in_specs = (
        P(("rep", *fs), None, None),
        P(),
        P(fs, tp),
        P(fs, tp),
        P(fs, tp),
        P(),
        P(fs, tp),
    )
    out_specs = P(("rep", *fs), None, tp)

    return jax.shard_map(local, mesh=fine, in_specs=in_specs, out_specs=out_specs, check_vma=False)
```

time: 131 us -> 143 us (1.092)
  the two profiles are of different devices: /device:TPU:1 before, /device:TPU:64 now
where the time goes in v2:
time: 143 us; the launch traced here: 142 us
  starting transfers between devices  84.3 us (59%)
  waiting for transfers between devices  44.3 us (31%)
  Pallas kernels  10.3 us (7%)
  local copies, waits for them, and re-layouts  2.72 us (2%)
    ppermute x16, starting transfers between devices, shift(): return lax.ppermute(x, axis, ring(size_of(axis), step))  57.1 us
    ppermute x16, waiting for transfers between devices, shift(): return lax.ppermute(x, axis, ring(size_of(axis), step))  44.3 us
    all_to_all x1, starting transfers between devices, exchange(): return lax.all_to_all(copies, axis, 0, 0, tiled=True)  15.7 us
    ppermute x4, starting transfers between devices, local(): other.append(lax.ppermute(g, 'core', [(0, 1), (1, 0)]))  8.64 us
  transfers between devices with their start and end apart: 22, of which 7 were waited for; matrix products, arithmetic and copies ran while one was open for 0% of the time, Pallas kernels for 4%

profile of v2, /device:TPU:64, one launch (start us, length us, event | category | flops | bytes accessed | tf_op | source)
XLA Modules:
  0.0 142.1 jit_solution(8043962496691520866)
XLA Ops:
  1.6 15.7 %all-to-all-start = ((bf16[4,64,768]{2,1,0:T(8,128)(2,1)}), bf16[4,64,768]{2,1,0:T(8,128)(2,1)S(1)}, u32[]{:S(2)}, u32[]{:S(2)}) async-start(bf16[4,64,768]{2,1,0:T(8,128)(2,1)} %shard_map.74), calls=%async_computation | async-start | bytes 786432 | tf_op jit(solution)/shard_map/all_to_all | solution.py:35
  17.3 3.4 %collective-permute-start.14 = (bf16[64,256]{1,0:T(8,128)(2,1)}, bf16[64,256]{1,0:T(8,128)(2,1)S(1)}, u32[]{:S(2)}, u32[]{:S(2)}) collective-permute-start(bf16[64,256]{1,0:T(8,128)(2,1)} %param.13), channel_id=1, source_target_pairs={{0,32},{32,64},{64,96},{96,128},{128,160},{160,192},{192,224},{224... | collective-permute-start | bytes 98312 | tf_op jit(solution)/shard_map/ppermute | solution.py:26
  20.7 2.5 %collective-permute-start.15 = (bf16[64,256]{1,0:T(8,128)(2,1)}, bf16[64,256]{1,0:T(8,128)(2,1)S(1)}, u32[]{:S(2)}, u32[]{:S(2)}) collective-permute-start(bf16[64,256]{1,0:T(8,128)(2,1)} %param.13), channel_id=1, source_target_pairs={{0,992},{32,0},{64,32},{96,64},{128,96},{160,128},{192,160},{224,1... | collective-permute-start | bytes 98312 | tf_op jit(solution)/shard_map/ppermute | solution.py:26
  25.1 2.8 %collective-permute-start = (bf16[4,64,768]{2,1,0:T(8,128)(2,1)S(1)}, bf16[4,64,768]{2,1,0:T(8,128)(2,1)S(1)}, u32[]{:S(2)}, u32[]{:S(2)}) collective-permute-start(bf16[4,64,768]{2,1,0:T(8,128)(2,1)S(1)} %all-to-all-done.refs_0_), channel_id=1, source_target_pairs={{0,992},{32,960},{64,160},{96,128},{128,96},{160,64},{192,288},{22... | collective-permute-start | bytes 1179656 | tf_op jit(solution)/shard_map/ppermute | solution.py:31
  32.7 6.0 %collective-permute-start.16 = (bf16[3,64,256]{2,1,0:T(8,128)(2,1)S(1)}, bf16[3,64,256]{2,1,0:T(8,128)(2,1)S(1)}, u32[]{:S(2)}, u32[]{:S(2)}) collective-permute-start(bf16[3,64,256]{2,1,0:T(8,128)(2,1)S(1)} %pad_maximum_fusion), channel_id=1, source_target_pairs={{0,96},{32,128},{64,160},{96,192},{128,224},{160,256},{192,288},{2... | collective-permute-start | bytes 294920 | tf_op jit(solution)/shard_map/ppermute | solution.py:26
  38.7 19.7 %collective-permute-done.16 = bf16[3,64,256]{2,1,0:T(8,128)(2,1)S(1)} collective-permute-done((bf16[3,64,256]{2,1,0:T(8,128)(2,1)S(1)}, bf16[3,64,256]{2,1,0:T(8,128)(2,1)S(1)}, u32[]{:S(2)}, u32[]{:S(2)}) %collective-permute-start.16) | collective-permute-done | bytes 98336 | tf_op jit(solution)/shard_map/ppermute | solution.py:26
  58.5 3.6 %collective-permute-start.5 = (bf16[4,64,768]{2,1,0:T(8,128)(2,1)S(1)}, bf16[4,64,768]{2,1,0:T(8,128)(2,1)S(1)}, u32[]{:S(2)}, u32[]{:S(2)}) collective-permute-start(bf16[4,64,768]{2,1,0:T(8,128)(2,1)S(1)} %all-to-all-done.refs_0_), channel_id=1, source_target_pairs={{0,24},{8,0},{16,8},{24,16},{1,25},{9,1},{17,9},{25,17},{2,26},{10... | collective-permute-start | bytes 1179656 | tf_op jit(solution)/shard_map/ppermute | solution.py:26
  62.1 3.8 %collective-permute-start.6 = (bf16[4,64,768]{2,1,0:T(8,128)(2,1)S(1)}, bf16[4,64,768]{2,1,0:T(8,128)(2,1)S(1)}, u32[]{:S(2)}, u32[]{:S(2)}) collective-permute-start(bf16[4,64,768]{2,1,0:T(8,128)(2,1)S(1)} %all-to-all-done.refs_0_), channel_id=1, source_target_pairs={{0,16},{8,24},{16,0},{24,8},{1,17},{9,25},{17,1},{25,9},{2,18},{10... | collective-permute-start | bytes 1179656 | tf_op jit(solution)/shard_map/ppermute | solution.py:26
  65.9 2.6 %collective-permute-start.1 = (bf16[4,64,768]{2,1,0:T(8,128)(2,1)S(1)}, bf16[4,64,768]{2,1,0:T(8,128)(2,1)S(1)}, u32[]{:S(2)}, u32[]{:S(2)}) collective-permute-start(bf16[4,64,768]{2,1,0:T(8,128)(2,1)S(1)} %collective-permute-done.refs_0_), channel_id=1, source_target_pairs={{0,8},{8,16},{16,24},{24,0},{1,9},{9,17},{17,25},{25,1},{2,10},{10... | collective-permute-start | bytes 1179656 | tf_op jit(solution)/shard_map/ppermute | solution.py:26
  68.5 4.5 %collective-permute-start.2 = (bf16[4,64,768]{2,1,0:T(8,128)(2,1)S(1)}, bf16[4,64,768]{2,1,0:T(8,128)(2,1)S(1)}, u32[]{:S(2)}, u32[]{:S(2)}) collective-permute-start(bf16[4,64,768]{2,1,0:T(8,128)(2,1)S(1)} %collective-permute-done.refs_0_), channel_id=1, source_target_pairs={{0,24},{8,0},{16,8},{24,16},{1,25},{9,1},{17,9},{25,17},{2,26},{10... | collective-permute-start | bytes 1179656 | tf_op jit(solution)/shard_map/ppermute | solution.py:26
  79.6 6.3 %collective-permute-done.1.refs_1_ = bf16[4,64,768]{2,1,0:T(8,128)(2,1)S(1)} collective-permute-done((bf16[4,64,768]{2,1,0:T(8,128)(2,1)S(1)}, bf16[4,64,768]{2,1,0:T(8,128)(2,1)S(1)}, u32[]{:S(2)}, u32[]{:S(2)}) %collective-permute-start.1) | collective-permute-done | bytes 393248 | tf_op jit(solution)/shard_map/ppermute | solution.py:26
  85.9 3.4 %collective-permute-done.2.refs_2_ = bf16[4,64,768]{2,1,0:T(8,128)(2,1)S(1)} collective-permute-done((bf16[4,64,768]{2,1,0:T(8,128)(2,1)S(1)}, bf16[4,64,768]{2,1,0:T(8,128)(2,1)S(1)}, u32[]{:S(2)}, u32[]{:S(2)}) %collective-permute-start.2) | collective-permute-done | bytes 393248 | tf_op jit(solution)/shard_map/ppermute | solution.py:26
  89.2 3.9 %collective-permute-done.3.refs_3_ = bf16[4,64,768]{2,1,0:T(8,128)(2,1)S(1)} collective-permute-done((bf16[4,64,768]{2,1,0:T(8,128)(2,1)S(1)}, bf16[4,64,768]{2,1,0:T(8,128)(2,1)S(1)}, u32[]{:S(2)}, u32[]{:S(2)}) %collective-permute-start.3) | collective-permute-done | bytes 393248 | tf_op jit(solution)/shard_map/ppermute | solution.py:26
  95.5 3.4 %collective-permute-start.7 = (bf16[768,256]{1,0:T(8,128)(2,1)S(1)}, bf16[768,256]{1,0:T(8,128)(2,1)S(1)}, u32[]{:S(2)}, u32[]{:S(2)}) collective-permute-start(bf16[768,256]{1,0:T(8,128)(2,1)S(1)} %shard_map.76.refs_0_), channel_id=1, source_target_pairs={{0,2},{2,4},{4,6},{6,0},{1,3},{3,5},{5,7},{7,1},{8,10},{10,12},{12... | collective-permute-start | bytes 1179656 | tf_op jit(solution)/shard_map/ppermute | solution.py:26
  98.9 3.7 %collective-permute-start.8 = (bf16[768,256]{1,0:T(8,128)(2,1)S(1)}, bf16[768,256]{1,0:T(8,128)(2,1)S(1)}, u32[]{:S(2)}, u32[]{:S(2)}) collective-permute-start(bf16[768,256]{1,0:T(8,128)(2,1)S(1)} %shard_map.76.refs_0_), channel_id=1, source_target_pairs={{0,6},{2,0},{4,2},{6,4},{1,7},{3,1},{5,3},{7,5},{8,14},{10,8},{12,... | collective-permute-start | bytes 1179656 | tf_op jit(solution)/shard_map/ppermute | solution.py:26
  102.6 3.7 %collective-permute-start.9 = (bf16[768,256]{1,0:T(8,128)(2,1)S(1)}, bf16[768,256]{1,0:T(8,128)(2,1)S(1)}, u32[]{:S(2)}, u32[]{:S(2)}) collective-permute-start(bf16[768,256]{1,0:T(8,128)(2,1)S(1)} %shard_map.76.refs_0_), channel_id=1, source_target_pairs={{0,4},{2,6},{4,0},{6,2},{1,5},{3,7},{5,1},{7,3},{8,12},{10,14},{12... | collective-permute-start | bytes 1179656 | tf_op jit(solution)/shard_map/ppermute | solution.py:26
  106.3 7.8 %collective-permute-start.18 = (bf16[8,64,256]{2,1,0:T(8,128)(2,1)S(1)}, bf16[8,64,256]{2,1,0:T(8,128)(2,1)S(1)}, u32[]{:S(2)}, u32[]{:S(2)}) collective-permute-start(bf16[8,64,256]{2,1,0:T(8,128)(2,1)S(1)} %constant_dynamic-update-slice_fusion.refs_8_), channel_id=1, source_target_pairs={{0,8},{8,16},{16,24},{24,0},{1,9},{9,17},{17,25},{25,1},{2,10},{10... | collective-permute-start | bytes 786440 | tf_op jit(solution)/shard_map/ppermute | solution.py:26
  114.1 2.5 %collective-permute-start.19 = (bf16[8,64,256]{2,1,0:T(8,128)(2,1)S(1)}, bf16[8,64,256]{2,1,0:T(8,128)(2,1)S(1)}, u32[]{:S(2)}, u32[]{:S(2)}) collective-permute-start(bf16[8,64,256]{2,1,0:T(8,128)(2,1)S(1)} %constant_dynamic-update-slice_fusion.refs_8_), channel_id=1, source_target_pairs={{0,24},{8,0},{16,8},{24,16},{1,25},{9,1},{17,9},{25,17},{2,26},{10... | collective-permute-start | bytes 786440 | tf_op jit(solution)/shard_map/ppermute | solution.py:26
  116.6 2.7 %collective-permute-done.18.refs_9_ = bf16[8,64,256]{2,1,0:T(8,128)(2,1)S(1)} collective-permute-done((bf16[8,64,256]{2,1,0:T(8,128)(2,1)S(1)}, bf16[8,64,256]{2,1,0:T(8,128)(2,1)S(1)}, u32[]{:S(2)}, u32[]{:S(2)}) %collective-permute-start.18) | collective-permute-done | bytes 262176 | tf_op jit(solution)/shard_map/ppermute | solution.py:26
  121.2 2.4 %collective-permute-start.11 = (bf16[768,256]{1,0:T(8,128)(2,1)S(1)}, bf16[768,256]{1,0:T(8,128)(2,1)S(1)}, u32[]{:S(2)}, u32[]{:S(2)}) collective-permute-start(bf16[768,256]{1,0:T(8,128)(2,1)S(1)} %collective-permute-done.7.refs_1_), channel_id=1, source_target_pairs={{0,1},{1,0},{2,3},{3,2},{4,5},{5,4},{6,7},{7,6},{8,9},{9,8},{10,11... | collective-permute-start | bytes 1179656 | tf_op jit(solution)/shard_map/ppermute | solution.py:205
  125.6 2.4 %collective-permute-start.13 = (bf16[768,256]{1,0:T(8,128)(2,1)S(1)}, bf16[768,256]{1,0:T(8,128)(2,1)S(1)}, u32[]{:S(2)}, u32[]{:S(2)}) collective-permute-start(bf16[768,256]{1,0:T(8,128)(2,1)S(1)} %collective-permute-done.9.refs_3_), channel_id=1, source_target_pairs={{0,1},{1,0},{2,3},{3,2},{4,5},{5,4},{6,7},{7,6},{8,9},{9,8},{10,11... | collective-permute-start | bytes 1179656 | tf_op jit(solution)/shard_map/ppermute | solution.py:205
  128.0 3.6 %collective-permute-start.20 = (bf16[8,64,256]{2,1,0:T(8,128)(2,1)S(1)}, bf16[8,64,256]{2,1,0:T(8,128)(2,1)S(1)}, u32[]{:S(2)}, u32[]{:S(2)}) collective-permute-start(bf16[8,64,256]{2,1,0:T(8,128)(2,1)S(1)} %constant_dynamic-update-slice_fusion.refs_8_), channel_id=1, source_target_pairs={{0,16},{8,24},{16,0},{24,8},{1,17},{9,25},{17,1},{25,9},{2,18},{10... | collective-permute-start | bytes 786440 | tf_op jit(solution)/shard_map/ppermute | solution.py:26
  131.6 8.1 %collective-permute-done.20.refs_11_ = bf16[8,64,256]{2,1,0:T(8,128)(2,1)S(1)} collective-permute-done((bf16[8,64,256]{2,1,0:T(8,128)(2,1)S(1)}, bf16[8,64,256]{2,1,0:T(8,128)(2,1)S(1)}, u32[]{:S(2)}, u32[]{:S(2)}) %collective-permute-start.20) | collective-permute-done | bytes 262176 | tf_op jit(solution)/shard_map/ppermute | solution.py:26
  139.7 2.4 %shard_map.77 = bf16[768,256]{1,0:T(8,128)(2,1)} custom-call(s32[5]{0:T(128)S(1)} %stack.37.at_ref, bf16[768,256]{1,0:T(8,128)(2,1)S(1)} %shard_map.76.refs_0_, bf16[768,256]{1,0:T(8,128)(2,1)S(1)} %collective-permute-done.7.refs_1_, bf16[768,256]{1,0:T(8,128)(2,1)S(1)} %collective-permute-done.8.refs_2_, ...), custom_call_target="tpu_custom_call" | custom-call | flops 805306368 | bytes 6291456 | tf_op jit(solution)/shard_map/pallas_call | solution.py:215
  (42 shorter events, 20.9 us)
Async XLA Ops:
  0.0 27.9 %copy-start = (f32[3,2048]{1,0:T(4,128)S(1)}, f32[3,2048]{1,0:T(4,128)}, u32[]{:S(2)}) copy-start(f32[3,2048]{1,0:T(4,128)} %param.12) | copy-start | bytes 73732
  1.6 21.6 %all-to-all-start = ((bf16[4,64,768]{2,1,0:T(8,128)(2,1)}), bf16[4,64,768]{2,1,0:T(8,128)(2,1)S(1)}, u32[]{:S(2)}, u32[]{:S(2)}) async-start(bf16[4,64,768]{2,1,0:T(8,128)(2,1)} %shard_map.74), calls=%async_computation | async-start | bytes 786432 | tf_op jit(solution)/shard_map/all_to_all | solution.py:35
  17.3 15.3 %collective-permute-start.14 = (bf16[64,256]{1,0:T(8,128)(2,1)}, bf16[64,256]{1,0:T(8,128)(2,1)S(1)}, u32[]{:S(2)}, u32[]{:S(2)}) collective-permute-start(bf16[64,256]{1,0:T(8,128)(2,1)} %param.13), channel_id=1, source_target_pairs={{0,32},{32,64},{64,96},{96,128},{128,160},{160,192},{192,224},{224... | collective-permute-start | bytes 98312 | tf_op jit(solution)/shard_map/ppermute | solution.py:26
  20.7 12.0 %collective-permute-start.15 = (bf16[64,256]{1,0:T(8,128)(2,1)}, bf16[64,256]{1,0:T(8,128)(2,1)S(1)}, u32[]{:S(2)}, u32[]{:S(2)}) collective-permute-start(bf16[64,256]{1,0:T(8,128)(2,1)} %param.13), channel_id=1, source_target_pairs={{0,992},{32,0},{64,32},{96,64},{128,96},{160,128},{192,160},{224,1... | collective-permute-start | bytes 98312 | tf_op jit(solution)/shard_map/ppermute | solution.py:26
  23.2 49.8 %collective-permute-start.4 = (bf16[4,64,768]{2,1,0:T(8,128)(2,1)S(1)}, bf16[4,64,768]{2,1,0:T(8,128)(2,1)S(1)}, u32[]{:S(2)}, u32[]{:S(2)}) collective-permute-start(bf16[4,64,768]{2,1,0:T(8,128)(2,1)S(1)} %all-to-all-done.refs_0_), channel_id=1, source_target_pairs={{0,8},{8,16},{16,24},{24,0},{1,9},{9,17},{17,25},{25,1},{2,10},{10... | collective-permute-start | bytes 1179656 | tf_op jit(solution)/shard_map/ppermute | solution.py:26
  25.1 40.8 %collective-permute-start = (bf16[4,64,768]{2,1,0:T(8,128)(2,1)S(1)}, bf16[4,64,768]{2,1,0:T(8,128)(2,1)S(1)}, u32[]{:S(2)}, u32[]{:S(2)}) collective-permute-start(bf16[4,64,768]{2,1,0:T(8,128)(2,1)S(1)} %all-to-all-done.refs_0_), channel_id=1, source_target_pairs={{0,992},{32,960},{64,160},{96,128},{128,96},{160,64},{192,288},{22... | collective-permute-start | bytes 1179656 | tf_op jit(solution)/shard_map/ppermute | solution.py:31
  30.6 2.0 %copy-start.3 = (bf16[64,256]{1,0:T(8,128)(2,1)S(1)}, bf16[64,256]{1,0:T(8,128)(2,1)}, u32[]{:S(2)}) copy-start(bf16[64,256]{1,0:T(8,128)(2,1)} %param.13) | copy-start | bytes 98308
  32.7 25.8 %collective-permute-start.16 = (bf16[3,64,256]{2,1,0:T(8,128)(2,1)S(1)}, bf16[3,64,256]{2,1,0:T(8,128)(2,1)S(1)}, u32[]{:S(2)}, u32[]{:S(2)}) collective-permute-start(bf16[3,64,256]{2,1,0:T(8,128)(2,1)S(1)} %pad_maximum_fusion), channel_id=1, source_target_pairs={{0,96},{32,128},{64,160},{96,192},{128,224},{160,256},{192,288},{2... | collective-permute-start | bytes 294920 | tf_op jit(solution)/shard_map/ppermute | solution.py:26
  58.5 16.9 %collective-permute-start.5 = (bf16[4,64,768]{2,1,0:T(8,128)(2,1)S(1)}, bf16[4,64,768]{2,1,0:T(8,128)(2,1)S(1)}, u32[]{:S(2)}, u32[]{:S(2)}) collective-permute-start(bf16[4,64,768]{2,1,0:T(8,128)(2,1)S(1)} %all-to-all-done.refs_0_), channel_id=1, source_target_pairs={{0,24},{8,0},{16,8},{24,16},{1,25},{9,1},{17,9},{25,17},{2,26},{10... | collective-permute-start | bytes 1179656 | tf_op jit(solution)/shard_map/ppermute | solution.py:26
  62.1 15.4 %collective-permute-start.6 = (bf16[4,64,768]{2,1,0:T(8,128)(2,1)S(1)}, bf16[4,64,768]{2,1,0:T(8,128)(2,1)S(1)}, u32[]{:S(2)}, u32[]{:S(2)}) collective-permute-start(bf16[4,64,768]{2,1,0:T(8,128)(2,1)S(1)} %all-to-all-done.refs_0_), channel_id=1, source_target_pairs={{0,16},{8,24},{16,0},{24,8},{1,17},{9,25},{17,1},{25,9},{2,18},{10... | collective-permute-start | bytes 1179656 | tf_op jit(solution)/shard_map/ppermute | solution.py:26
  65.9 19.9 %collective-permute-start.1 = (bf16[4,64,768]{2,1,0:T(8,128)(2,1)S(1)}, bf16[4,64,768]{2,1,0:T(8,128)(2,1)S(1)}, u32[]{:S(2)}, u32[]{:S(2)}) collective-permute-start(bf16[4,64,768]{2,1,0:T(8,128)(2,1)S(1)} %collective-permute-done.refs_0_), channel_id=1, source_target_pairs={{0,8},{8,16},{16,24},{24,0},{1,9},{9,17},{17,25},{25,1},{2,10},{10... | collective-permute-start | bytes 1179656 | tf_op jit(solution)/shard_map/ppermute | solution.py:26
  68.5 20.7 %collective-permute-start.2 = (bf16[4,64,768]{2,1,0:T(8,128)(2,1)S(1)}, bf16[4,64,768]{2,1,0:T(8,128)(2,1)S(1)}, u32[]{:S(2)}, u32[]{:S(2)}) collective-permute-start(bf16[4,64,768]{2,1,0:T(8,128)(2,1)S(1)} %collective-permute-done.refs_0_), channel_id=1, source_target_pairs={{0,24},{8,0},{16,8},{24,16},{1,25},{9,1},{17,9},{25,17},{2,26},{10... | collective-permute-start | bytes 1179656 | tf_op jit(solution)/shard_map/ppermute | solution.py:26
  73.0 20.1 %collective-permute-start.3 = (bf16[4,64,768]{2,1,0:T(8,128)(2,1)S(1)}, bf16[4,64,768]{2,1,0:T(8,128)(2,1)S(1)}, u32[]{:S(2)}, u32[]{:S(2)}) collective-permute-start(bf16[4,64,768]{2,1,0:T(8,128)(2,1)S(1)} %collective-permute-done.refs_0_), channel_id=1, source_target_pairs={{0,16},{8,24},{16,0},{24,8},{1,17},{9,25},{17,1},{25,9},{2,18},{10... | collective-permute-start | bytes 1179656 | tf_op jit(solution)/shard_map/ppermute | solution.py:26
  75.4 30.9 %collective-permute-start.17 = (bf16[2,64,256]{2,1,0:T(8,128)(2,1)S(1)}, bf16[2,64,256]{2,1,0:T(8,128)(2,1)S(1)}, u32[]{:S(2)}, u32[]{:S(2)}) collective-permute-start(bf16[2,64,256]{2,1,0:T(8,128)(2,1)S(1)} %pad_maximum_fusion.1), channel_id=1, source_target_pairs={{0,928},{32,960},{64,992},{96,0},{128,32},{160,64},{192,96},{224,1... | collective-permute-start | bytes 196616 | tf_op jit(solution)/shard_map/ppermute | solution.py:26
  95.5 25.7 %collective-permute-start.7 = (bf16[768,256]{1,0:T(8,128)(2,1)S(1)}, bf16[768,256]{1,0:T(8,128)(2,1)S(1)}, u32[]{:S(2)}, u32[]{:S(2)}) collective-permute-start(bf16[768,256]{1,0:T(8,128)(2,1)S(1)} %shard_map.76.refs_0_), channel_id=1, source_target_pairs={{0,2},{2,4},{4,6},{6,0},{1,3},{3,5},{5,7},{7,1},{8,10},{10,12},{12... | collective-permute-start | bytes 1179656 | tf_op jit(solution)/shard_map/ppermute | solution.py:26
  98.9 24.7 %collective-permute-start.8 = (bf16[768,256]{1,0:T(8,128)(2,1)S(1)}, bf16[768,256]{1,0:T(8,128)(2,1)S(1)}, u32[]{:S(2)}, u32[]{:S(2)}) collective-permute-start(bf16[768,256]{1,0:T(8,128)(2,1)S(1)} %shard_map.76.refs_0_), channel_id=1, source_target_pairs={{0,6},{2,0},{4,2},{6,4},{1,7},{3,1},{5,3},{7,5},{8,14},{10,8},{12,... | collective-permute-start | bytes 1179656 | tf_op jit(solution)/shard_map/ppermute | solution.py:26
  102.6 23.0 %collective-permute-start.9 = (bf16[768,256]{1,0:T(8,128)(2,1)S(1)}, bf16[768,256]{1,0:T(8,128)(2,1)S(1)}, u32[]{:S(2)}, u32[]{:S(2)}) collective-permute-start(bf16[768,256]{1,0:T(8,128)(2,1)S(1)} %shard_map.76.refs_0_), channel_id=1, source_target_pairs={{0,4},{2,6},{4,0},{6,2},{1,5},{3,7},{5,1},{7,3},{8,12},{10,14},{12... | collective-permute-start | bytes 1179656 | tf_op jit(solution)/shard_map/ppermute | solution.py:26
  106.3 13.0 %collective-permute-start.18 = (bf16[8,64,256]{2,1,0:T(8,128)(2,1)S(1)}, bf16[8,64,256]{2,1,0:T(8,128)(2,1)S(1)}, u32[]{:S(2)}, u32[]{:S(2)}) collective-permute-start(bf16[8,64,256]{2,1,0:T(8,128)(2,1)S(1)} %constant_dynamic-update-slice_fusion.refs_8_), channel_id=1, source_target_pairs={{0,8},{8,16},{16,24},{24,0},{1,9},{9,17},{17,25},{25,1},{2,10},{10... | collective-permute-start | bytes 786440 | tf_op jit(solution)/shard_map/ppermute | solution.py:26
  114.1 13.9 %collective-permute-start.19 = (bf16[8,64,256]{2,1,0:T(8,128)(2,1)S(1)}, bf16[8,64,256]{2,1,0:T(8,128)(2,1)S(1)}, u32[]{:S(2)}, u32[]{:S(2)}) collective-permute-start(bf16[8,64,256]{2,1,0:T(8,128)(2,1)S(1)} %constant_dynamic-update-slice_fusion.refs_8_), channel_id=1, source_target_pairs={{0,24},{8,0},{16,8},{24,16},{1,25},{9,1},{17,9},{25,17},{2,26},{10... | collective-permute-start | bytes 786440 | tf_op jit(solution)/shard_map/ppermute | solution.py:26
  119.3 20.3 %collective-permute-start.10 = (bf16[768,256]{1,0:T(8,128)(2,1)S(1)}, bf16[768,256]{1,0:T(8,128)(2,1)S(1)}, u32[]{:S(2)}, u32[]{:S(2)}) collective-permute-start(bf16[768,256]{1,0:T(8,128)(2,1)S(1)} %shard_map.76.refs_0_), channel_id=1, source_target_pairs={{0,1},{1,0},{2,3},{3,2},{4,5},{5,4},{6,7},{7,6},{8,9},{9,8},{10,11... | collective-permute-start | bytes 1179656 | tf_op jit(solution)/shard_map/ppermute | solution.py:205
  121.2 18.4 %collective-permute-start.11 = (bf16[768,256]{1,0:T(8,128)(2,1)S(1)}, bf16[768,256]{1,0:T(8,128)(2,1)S(1)}, u32[]{:S(2)}, u32[]{:S(2)}) collective-permute-start(bf16[768,256]{1,0:T(8,128)(2,1)S(1)} %collective-permute-done.7.refs_1_), channel_id=1, source_target_pairs={{0,1},{1,0},{2,3},{3,2},{4,5},{5,4},{6,7},{7,6},{8,9},{9,8},{10,11... | collective-permute-start | bytes 1179656 | tf_op jit(solution)/shard_map/ppermute | solution.py:205
  123.7 16.0 %collective-permute-start.12 = (bf16[768,256]{1,0:T(8,128)(2,1)S(1)}, bf16[768,256]{1,0:T(8,128)(2,1)S(1)}, u32[]{:S(2)}, u32[]{:S(2)}) collective-permute-start(bf16[768,256]{1,0:T(8,128)(2,1)S(1)} %collective-permute-done.8.refs_2_), channel_id=1, source_target_pairs={{0,1},{1,0},{2,3},{3,2},{4,5},{5,4},{6,7},{7,6},{8,9},{9,8},{10,11... | collective-permute-start | bytes 1179656 | tf_op jit(solution)/shard_map/ppermute | solution.py:205
  125.6 14.1 %collective-permute-start.13 = (bf16[768,256]{1,0:T(8,128)(2,1)S(1)}, bf16[768,256]{1,0:T(8,128)(2,1)S(1)}, u32[]{:S(2)}, u32[]{:S(2)}) collective-permute-start(bf16[768,256]{1,0:T(8,128)(2,1)S(1)} %collective-permute-done.9.refs_3_), channel_id=1, source_target_pairs={{0,1},{1,0},{2,3},{3,2},{4,5},{5,4},{6,7},{7,6},{8,9},{9,8},{10,11... | collective-permute-start | bytes 1179656 | tf_op jit(solution)/shard_map/ppermute | solution.py:205
  128.0 11.6 %collective-permute-start.20 = (bf16[8,64,256]{2,1,0:T(8,128)(2,1)S(1)}, bf16[8,64,256]{2,1,0:T(8,128)(2,1)S(1)}, u32[]{:S(2)}, u32[]{:S(2)}) collective-permute-start(bf16[8,64,256]{2,1,0:T(8,128)(2,1)S(1)} %constant_dynamic-update-slice_fusion.refs_8_), channel_id=1, source_target_pairs={{0,16},{8,24},{16,0},{24,8},{1,17},{9,25},{17,1},{25,9},{2,18},{10... | collective-permute-start | bytes 786440 | tf_op jit(solution)/shard_map/ppermute | solution.py:26
  (2 other events, 2.6 us)

commit v3 on v2

--- a/solution.py
+++ b/solution.py
@@ -49,18 +49,29 @@
             out_ref[p, :, k * columns : (k + 1) * columns] = held[k]
 
 
-def norm_kernel(x_ref, gain_ref, out_ref):
-    rows = 64
+def norm_kernel(x_ref, gain_ref, out_ref, held, sems):
+    rows = held.shape[1]
+    chunks = x_ref.shape[0] // rows
     gain = gain_ref[...]
-
-    def step(i, _):
-        at = pl.ds(pl.multiple_of(i * rows, rows), rows)
-        x = x_ref[at, :].astype(jnp.float32)
-        scale = lax.rsqrt(jnp.mean(x * x, axis=-1, keepdims=True) + 1e-06)
-        out_ref[at, :] = (x * scale * gain).astype(jnp.bfloat16)
-        return 0
-
-    lax.fori_loop(0, x_ref.shape[0] // rows, step, 0)
+    small = 32
+
+    def fetch(i):
+        return pltpu.make_async_copy(x_ref.at[pl.ds(i * rows, rows)], held.at[i % 2], sems.at[i % 2])
+
+    fetch(0).start()
+    for i in range(chunks):
+        if i + 1 < chunks:
+            fetch(i + 1).start()
+        fetch(i).wait()
+
+        def step(j, _, i=i):
+            at = pl.multiple_of(j * small, small)
+            x = held[i % 2, pl.ds(at, small), :].astype(jnp.float32)
+            scale = lax.rsqrt(jnp.mean(x * x, axis=-1, keepdims=True) + 1e-06)
+            out_ref[pl.ds(i * rows + at, small), :] = (x * scale * gain).astype(jnp.bfloat16)
+            return 0
+
+        lax.fori_loop(0, rows // small, step, 0)
 
 
 ROWS = 256
@@ -90,7 +101,7 @@
 def gate_kernel(at_ref, normed_ref, *refs):
     pieces, total_ref, taps_ref, out_ref, weight, product = refs[:4], *refs[4:]
     place_rows(at_ref, pieces, weight)
-    seq, columns = out_ref.shape
+    seq, columns = out_ref.shape[1:]
     product[0:8, :] = jnp.zeros((8, columns), jnp.float32)
     for r in range(0, seq, ROWS):
         parts = total_ref[r : r + ROWS, :] + half_dot(normed_ref, weight, 1 - at_ref[0], r)
@@ -100,36 +111,48 @@
         convolved = taps_ref[0:1, :] * product[6 + r : 6 + r + ROWS, :]
         convolved = convolved + taps_ref[1:2, :] * product[7 + r : 7 + r + ROWS, :]
         convolved = convolved + taps_ref[2:3, :] * product[8 + r : 8 + r + ROWS, :]
-        out_ref[r : r + ROWS, :] = (outer * convolved).astype(jnp.bfloat16)
-
-
-def out_kernel(at_ref, *refs):
-    gated, pieces, out_ref, weight = refs[:8], refs[8:12], refs[12], refs[13]
-    z, x, core, y = at_ref[1], at_ref[2], at_ref[3], at_ref[4]
-    for side in range(2):
-        for k, step in enumerate(STEPS):
-            tile = 2 * lax.rem(x + step + 4, 4) + lax.rem(core + side, 2)
-            offset = lax.rem(tile - z + 12, 8)
-            for piece, other in zip(pieces, STEPS):
-                at = (side * 4 + k) * 256 + lax.rem(y + other + 4, 4) * 64
-                weight[pl.ds(pl.multiple_of(at, 64), 64), :] = piece[offset]
+        gated = (outer * convolved).astype(jnp.bfloat16)
+        for p in range(out_ref.shape[0]):
+            out_ref[p, r : r + ROWS, :] = gated
+
+
+def side_dot(gated_ref, weight, r):
+    left = jnp.concatenate([gated_ref[k, r : r + ROWS, :] for k in range(gated_ref.shape[0])], axis=1)
+    return jnp.dot(left, weight, preferred_element_type=jnp.float32)
+
+
+def own_kernel(at_ref, gated_ref, *refs):
+    pieces, total_ref, rest_ref, weight = refs[:4], refs[4], refs[5], refs[6]
+    z, core, y = at_ref[1], at_ref[3], at_ref[4]
+    for side, target in enumerate((weight, rest_ref)):
+        for k in range(gated_ref.shape[0]):
+            offset = lax.rem(2 * k + lax.rem(core + side, 2) - z + 12, 8)
+            for piece, step in zip(pieces, STEPS):
+                at = k * 256 + lax.rem(y + step + 4, 4) * 64
+                target[pl.ds(pl.multiple_of(at, 64), 64), :] = piece[offset]
+    for r in range(0, total_ref.shape[0], ROWS):
+        total_ref[r : r + ROWS, :] = side_dot(gated_ref, weight[...], r)
+
+
+def other_kernel(gated_ref, rest_ref, total_ref, out_ref):
     for r in range(0, out_ref.shape[0], ROWS):
-        left = jnp.concatenate([g[r : r + ROWS, :] for g in gated], axis=1)
-        total = jnp.dot(left, weight[...], preferred_element_type=jnp.float32)
+        total = total_ref[r : r + ROWS, :] + side_dot(gated_ref, rest_ref[...], r)
         out_ref[r : r + ROWS, :] = total.astype(jnp.bfloat16)
 
 
 VMEM = pl.BlockSpec(memory_space=pltpu.VMEM)
+HBM = pl.BlockSpec(memory_space=pltpu.HBM)
 ANY = pl.BlockSpec(memory_space=pl.ANY)
 SMEM = pl.BlockSpec(memory_space=pltpu.SMEM)
 
 
 def call(kernel, shape, dtype, in_specs, flops, moved, scratch=(), limit=24):
+    shapes = [jax.ShapeDtypeStruct(*pair) for pair in zip(shape, dtype)] if isinstance(dtype, tuple) else None
     return pl.pallas_call(
         kernel,
-        out_shape=jax.ShapeDtypeStruct(shape, dtype),
+        out_shape=shapes or jax.ShapeDtypeStruct(shape, dtype),
         in_specs=in_specs,
-        out_specs=VMEM,
+        out_specs=[VMEM] * len(shapes) if shapes else VMEM,
         scratch_shapes=list(scratch),
         cost_estimate=pl.CostEstimate(flops=flops, bytes_accessed=moved, transcendentals=0),
         compiler_params=pltpu.CompilerParams(vmem_limit_bytes=limit << 20),
@@ -175,13 +198,20 @@
     other_group = mirror(group)
     near = pieces_of(group, "y")
 
-    norm = call(norm_kernel, (seq, width), bf16, [VMEM] * 2, 8 * seq * width, 4 * seq * width)
+    norm = call(
+        norm_kernel,
+        (seq, width),
+        bf16,
+        [HBM, VMEM],
+        8 * seq * width,
+        4 * seq * width,
+        [pltpu.VMEM((2, 192, width), bf16), pltpu.SemaphoreType.DMA((2,))],
+        limit=9,
+    )
     normed = norm(tokens.reshape(seq, width), norm_gain.reshape(1, width))
     flops = 3 * seq * width * columns
     weight = pltpu.VMEM((width // 2, 3 * columns), bf16)
-    start = call(
-        near_kernel, (seq, 3 * columns), f32, [SMEM] + [VMEM] * 5, flops, 8 * seq * width, [weight]
-    )
+    start = call(near_kernel, (seq, 3 * columns), f32, [SMEM] + [VMEM] * 5, flops, 8 * seq * width, [weight])
     total = start(place, normed, *near)
     far = pieces_of(other_group, "y")
 
@@ -189,7 +219,7 @@
     taps = lax.dynamic_slice_in_dim(conv_taps, (2 * x + core) * columns, columns, 1)
     gate = call(
         gate_kernel,
-        (seq, columns),
+        (lax.axis_size("x"), seq, columns),
         bf16,
         [SMEM] + [VMEM] * 7,
         flops,
@@ -199,20 +229,21 @@
     rows = pieces_of(out_rows, "y")
     gated = gate(place, normed, *far, total, taps)
 
-    own = pieces_of(gated, "x")
-    other = []
-    for g in own:
-        other.append(lax.ppermute(g, "core", [(0, 1), (1, 0)]))
-    project = call(
-        out_kernel,
-        (seq, columns),
-        bf16,
-        [SMEM] + [VMEM] * 12,
-        2 * seq * width * columns,
+    own = exchange(gated, "x")
+    other = lax.ppermute(own, "core", [(0, 1), (1, 0)])
+    flops = seq * width * columns
+    first = call(
+        own_kernel,
+        ((seq, columns), (width // 2, columns)),
+        (f32, bf16),
+        [SMEM] + [VMEM] * 5,
+        flops,
         4 * seq * width,
-        [pltpu.VMEM((width, columns), bf16)],
-    )
-    return project(place, *own, *other, *rows).reshape(1, seq, columns)
+        [pltpu.VMEM((width // 2, columns), bf16)],
+    )
+    total, rest = first(place, own, *rows)
+    last = call(other_kernel, (seq, columns), bf16, [VMEM] * 3, flops, 4 * seq * width)
+    return last(other, rest, total).reshape(1, seq, columns)
 
 
 def solution(mesh):

time: 143 us -> 147 us (1.028)
  the two profiles are of different devices: /device:TPU:64 before, /device:TPU:8 now
where the time goes in v3:
time: 147 us; the launch traced here: 146 us
  starting transfers between devices  63 us (43%)
  blocking collectives  41.4 us (28%)
  waiting for transfers between devices  26.5 us (18%)
  Pallas kernels  12 us (8%)
  local copies, waits for them, and re-layouts  2.72 us (2%)
    ppermute x13, starting transfers between devices, shift(): return lax.ppermute(x, axis, ring(size_of(axis), step))  45 us
    all_to_all x2, blocking collectives, exchange(): return lax.all_to_all(copies, axis, 0, 0, tiled=True)  41.4 us
    ppermute x13, waiting for transfers between devices, shift(): return lax.ppermute(x, axis, ring(size_of(axis), step))  20.2 us
    ppermute x1, starting transfers between devices, mirror(): lax.ppermute(x, LINE, [(i, (i + (-1, -3, 3, 1)[i % 4]) % size) for i in r...  16 us
    ppermute x1, waiting for transfers between devices, mirror(): lax.ppermute(x, LINE, [(i, (i + (-1, -3, 3, 1)[i % 4]) % size) for i in r...  6.3 us
    pallas_call x1, Pallas kernels, local(): normed = norm(tokens.reshape(seq, width), norm_gain.reshape(1, width))  3.43 us
  transfers between devices with their start and end apart: 15, of which 8 were waited for; matrix products, arithmetic and copies ran while one was open for 0% of the time, Pallas kernels for 5%

profile of v3, /device:TPU:8, one launch (start us, length us, event | category | flops | bytes accessed | tf_op | source)
XLA Modules:
  0.0 145.9 jit_solution(15030576880220210473)
XLA Ops:
  1.6 17.6 %all_to_all.10.refs_0_ = bf16[4,64,768]{2,1,0:T(8,128)(2,1)S(1)} all-to-all(bf16[4,64,768]{2,1,0:T(8,128)(2,1)} %shard_map.74), channel_id=1, replica_groups=mesh['rep'=4,'zh'=2,'zl'=4,'y'=4,'x'=4,'core'=2] {'zl'}, dimensions={0} | all-to-all | bytes 786432 | tf_op jit(solution)/shard_map/all_to_all | solution.py:35
  19.2 16.0 %collective-permute-start = (bf16[4,64,768]{2,1,0:T(8,128)(2,1)S(1)}, bf16[4,64,768]{2,1,0:T(8,128)(2,1)S(1)}, u32[]{:S(2)}, u32[]{:S(2)}) collective-permute-start(bf16[4,64,768]{2,1,0:T(8,128)(2,1)S(1)} %all_to_all.10.refs_0_), channel_id=1, source_target_pairs={{0,992},{32,960},{64,160},{96,128},{128,96},{160,64},{192,288},{22... | collective-permute-start | bytes 1179656 | tf_op jit(solution)/shard_map/ppermute | solution.py:31
  35.2 3.5 %collective-permute-start.4 = (bf16[4,64,768]{2,1,0:T(8,128)(2,1)S(1)}, bf16[4,64,768]{2,1,0:T(8,128)(2,1)S(1)}, u32[]{:S(2)}, u32[]{:S(2)}) collective-permute-start(bf16[4,64,768]{2,1,0:T(8,128)(2,1)S(1)} %all_to_all.10.refs_0_), channel_id=1, source_target_pairs={{0,8},{8,16},{16,24},{24,0},{1,9},{9,17},{17,25},{25,1},{2,10},{10... | collective-permute-start | bytes 1179656 | tf_op jit(solution)/shard_map/ppermute | solution.py:26
  38.7 2.4 %collective-permute-start.5 = (bf16[4,64,768]{2,1,0:T(8,128)(2,1)S(1)}, bf16[4,64,768]{2,1,0:T(8,128)(2,1)S(1)}, u32[]{:S(2)}, u32[]{:S(2)}) collective-permute-start(bf16[4,64,768]{2,1,0:T(8,128)(2,1)S(1)} %all_to_all.10.refs_0_), channel_id=1, source_target_pairs={{0,24},{8,0},{16,8},{24,16},{1,25},{9,1},{17,9},{25,17},{2,26},{10... | collective-permute-start | bytes 1179656 | tf_op jit(solution)/shard_map/ppermute | solution.py:26
  41.0 4.2 %collective-permute-start.6 = (bf16[4,64,768]{2,1,0:T(8,128)(2,1)S(1)}, bf16[4,64,768]{2,1,0:T(8,128)(2,1)S(1)}, u32[]{:S(2)}, u32[]{:S(2)}) collective-permute-start(bf16[4,64,768]{2,1,0:T(8,128)(2,1)S(1)} %all_to_all.10.refs_0_), channel_id=1, source_target_pairs={{0,16},{8,24},{16,0},{24,8},{1,17},{9,25},{17,1},{25,9},{2,18},{10... | collective-permute-start | bytes 1179656 | tf_op jit(solution)/shard_map/ppermute | solution.py:26
  45.3 6.3 %collective-permute-done.refs_0_ = bf16[4,64,768]{2,1,0:T(8,128)(2,1)S(1)} collective-permute-done((bf16[4,64,768]{2,1,0:T(8,128)(2,1)S(1)}, bf16[4,64,768]{2,1,0:T(8,128)(2,1)S(1)}, u32[]{:S(2)}, u32[]{:S(2)}) %collective-permute-start) | collective-permute-done | bytes 393248 | tf_op jit(solution)/shard_map/ppermute | solution.py:31
  51.6 3.5 %collective-permute-start.1 = (bf16[4,64,768]{2,1,0:T(8,128)(2,1)S(1)}, bf16[4,64,768]{2,1,0:T(8,128)(2,1)S(1)}, u32[]{:S(2)}, u32[]{:S(2)}) collective-permute-start(bf16[4,64,768]{2,1,0:T(8,128)(2,1)S(1)} %collective-permute-done.refs_0_), channel_id=1, source_target_pairs={{0,8},{8,16},{16,24},{24,0},{1,9},{9,17},{17,25},{25,1},{2,10},{10... | collective-permute-start | bytes 1179656 | tf_op jit(solution)/shard_map/ppermute | solution.py:26
  55.0 2.4 %collective-permute-start.2 = (bf16[4,64,768]{2,1,0:T(8,128)(2,1)S(1)}, bf16[4,64,768]{2,1,0:T(8,128)(2,1)S(1)}, u32[]{:S(2)}, u32[]{:S(2)}) collective-permute-start(bf16[4,64,768]{2,1,0:T(8,128)(2,1)S(1)} %collective-permute-done.refs_0_), channel_id=1, source_target_pairs={{0,24},{8,0},{16,8},{24,16},{1,25},{9,1},{17,9},{25,17},{2,26},{10... | collective-permute-start | bytes 1179656 | tf_op jit(solution)/shard_map/ppermute | solution.py:26
  57.4 4.2 %collective-permute-start.3 = (bf16[4,64,768]{2,1,0:T(8,128)(2,1)S(1)}, bf16[4,64,768]{2,1,0:T(8,128)(2,1)S(1)}, u32[]{:S(2)}, u32[]{:S(2)}) collective-permute-start(bf16[4,64,768]{2,1,0:T(8,128)(2,1)S(1)} %collective-permute-done.refs_0_), channel_id=1, source_target_pairs={{0,16},{8,24},{16,0},{24,8},{1,17},{9,25},{17,1},{25,9},{2,18},{10... | collective-permute-start | bytes 1179656 | tf_op jit(solution)/shard_map/ppermute | solution.py:26
  64.3 3.4 %shard_map.73.normed_ref = bf16[768,2048]{1,0:T(8,128)(2,1)S(1)} custom-call(bf16[768,2048]{1,0:T(8,128)(2,1)S(1)} %bitcast.14, f32[1,2048]{1,0:T(1,128)S(1)} %bitcast.15), custom_call_target="tpu_custom_call" | custom-call | flops 12582912 | bytes 6291456 | tf_op jit(solution)/shard_map/pallas_call | solution.py:211
  67.8 2.0 %shard_map.75.refs_4_ = f32[768,768]{1,0:T(8,128)S(1)} custom-call(s32[5]{0:T(128)S(1)} %stack.37.at_ref, bf16[768,2048]{1,0:T(8,128)(2,1)S(1)} %shard_map.73.normed_ref, bf16[4,64,768]{2,1,0:T(8,128)(2,1)S(1)} %all_to_all.10.refs_0_, bf16[4,64,768]{2,1,0:T(8,128)(2,1)S(1)} %collective-permute-done.4.refs_1_, ...), custom_call_target="tpu_custom_call" | custom-call | flops 1207959552 | bytes 12582912 | tf_op jit(solution)/shard_map/pallas_call | solution.py:215
  69.9 7.0 %collective-permute-done.3.refs_3_ = bf16[4,64,768]{2,1,0:T(8,128)(2,1)S(1)} collective-permute-done((bf16[4,64,768]{2,1,0:T(8,128)(2,1)S(1)}, bf16[4,64,768]{2,1,0:T(8,128)(2,1)S(1)}, u32[]{:S(2)}, u32[]{:S(2)}) %collective-permute-start.3) | collective-permute-done | bytes 393248 | tf_op jit(solution)/shard_map/ppermute | solution.py:26
  76.8 2.4 %shard_map.76 = bf16[4,768,256]{2,1,0:T(8,128)(2,1)S(1)} custom-call(s32[5]{0:T(128)S(1)} %stack.37.at_ref, bf16[768,2048]{1,0:T(8,128)(2,1)S(1)} %shard_map.73.normed_ref, bf16[4,64,768]{2,1,0:T(8,128)(2,1)S(1)} %collective-permute-done.refs_0_, bf16[4,64,768]{2,1,0:T(8,128)(2,1)S(1)} %collective-permute-done.1.refs_1_, ...), custom_call_target="tpu_custom_call" | custom-call | flops 1207959552 | bytes 12582912 | tf_op jit(solution)/shard_map/pallas_call | solution.py:230
  79.3 23.9 %all_to_all.11.gated_ref = bf16[4,768,256]{2,1,0:T(8,128)(2,1)S(1)} all-to-all(bf16[4,768,256]{2,1,0:T(8,128)(2,1)S(1)} %shard_map.76), channel_id=1, replica_groups=mesh['rep'=4,'zh'=2,'zl'=4,'y'=4,'x'=4,'core'=2] {'x'}, dimensions={0} | all-to-all | bytes 3145728 | tf_op jit(solution)/shard_map/all_to_all | solution.py:35
  103.1 1.9 %collective-permute-start.7 = (bf16[4,768,256]{2,1,0:T(8,128)(2,1)S(1)}, bf16[4,768,256]{2,1,0:T(8,128)(2,1)S(1)}, u32[]{:S(2)}, u32[]{:S(2)}) collective-permute-start(bf16[4,768,256]{2,1,0:T(8,128)(2,1)S(1)} %all_to_all.11.gated_ref), channel_id=1, source_target_pairs={{0,1},{1,0},{2,3},{3,2},{4,5},{5,4},{6,7},{7,6},{8,9},{9,8},{10,11... | collective-permute-start | bytes 4718600 | tf_op jit(solution)/shard_map/ppermute | solution.py:233
  105.0 1.9 %collective-permute-start.8 = (bf16[64,256]{1,0:T(8,128)(2,1)S(1)}, bf16[64,256]{1,0:T(8,128)(2,1)S(1)}, u32[]{:S(2)}, u32[]{:S(2)}) collective-permute-start(bf16[64,256]{1,0:T(8,128)(2,1)S(1)} %copy-done.3), channel_id=1, source_target_pairs={{0,32},{32,64},{64,96},{96,128},{128,160},{160,192},{192,224},{224... | collective-permute-start | bytes 98312 | tf_op jit(solution)/shard_map/ppermute | solution.py:26
  107.0 5.2 %collective-permute-start.9 = (bf16[64,256]{1,0:T(8,128)(2,1)S(1)}, bf16[64,256]{1,0:T(8,128)(2,1)S(1)}, u32[]{:S(2)}, u32[]{:S(2)}) collective-permute-start(bf16[64,256]{1,0:T(8,128)(2,1)S(1)} %copy-done.3), channel_id=1, source_target_pairs={{0,992},{32,0},{64,32},{96,64},{128,96},{160,128},{192,160},{224,1... | collective-permute-start | bytes 98312 | tf_op jit(solution)/shard_map/ppermute | solution.py:26
  113.7 1.9 %collective-permute-start.10 = (bf16[3,64,256]{2,1,0:T(8,128)(2,1)S(1)}, bf16[3,64,256]{2,1,0:T(8,128)(2,1)S(1)}, u32[]{:S(2)}, u32[]{:S(2)}) collective-permute-start(bf16[3,64,256]{2,1,0:T(8,128)(2,1)S(1)} %pad_maximum_fusion), channel_id=1, source_target_pairs={{0,96},{32,128},{64,160},{96,192},{128,224},{160,256},{192,288},{2... | collective-permute-start | bytes 294920 | tf_op jit(solution)/shard_map/ppermute | solution.py:26
  115.7 6.9 %collective-permute-start.11 = (bf16[2,64,256]{2,1,0:T(8,128)(2,1)S(1)}, bf16[2,64,256]{2,1,0:T(8,128)(2,1)S(1)}, u32[]{:S(2)}, u32[]{:S(2)}) collective-permute-start(bf16[2,64,256]{2,1,0:T(8,128)(2,1)S(1)} %pad_maximum_fusion.1), channel_id=1, source_target_pairs={{0,928},{32,960},{64,992},{96,0},{128,32},{160,64},{192,96},{224,1... | collective-permute-start | bytes 196616 | tf_op jit(solution)/shard_map/ppermute | solution.py:26
  124.4 1.9 %collective-permute-done.11 = bf16[2,64,256]{2,1,0:T(8,128)(2,1)S(1)} collective-permute-done((bf16[2,64,256]{2,1,0:T(8,128)(2,1)S(1)}, bf16[2,64,256]{2,1,0:T(8,128)(2,1)S(1)}, u32[]{:S(2)}, u32[]{:S(2)}) %collective-permute-start.11) | collective-permute-done | bytes 65568 | tf_op jit(solution)/shard_map/ppermute | solution.py:26
  128.2 3.9 %collective-permute-start.13 = (bf16[8,64,256]{2,1,0:T(8,128)(2,1)S(1)}, bf16[8,64,256]{2,1,0:T(8,128)(2,1)S(1)}, u32[]{:S(2)}, u32[]{:S(2)}) collective-permute-start(bf16[8,64,256]{2,1,0:T(8,128)(2,1)S(1)} %constant_dynamic-update-slice_fusion.refs_0_), channel_id=1, source_target_pairs={{0,24},{8,0},{16,8},{24,16},{1,25},{9,1},{17,9},{25,17},{2,26},{10... | collective-permute-start | bytes 786440 | tf_op jit(solution)/shard_map/ppermute | solution.py:26
  132.1 3.2 %collective-permute-start.14 = (bf16[8,64,256]{2,1,0:T(8,128)(2,1)S(1)}, bf16[8,64,256]{2,1,0:T(8,128)(2,1)S(1)}, u32[]{:S(2)}, u32[]{:S(2)}) collective-permute-start(bf16[8,64,256]{2,1,0:T(8,128)(2,1)S(1)} %constant_dynamic-update-slice_fusion.refs_0_), channel_id=1, source_target_pairs={{0,16},{8,24},{16,0},{24,8},{1,17},{9,25},{17,1},{25,9},{2,18},{10... | collective-permute-start | bytes 786440 | tf_op jit(solution)/shard_map/ppermute | solution.py:26
  135.4 3.3 %collective-permute-done.13.refs_2_ = bf16[8,64,256]{2,1,0:T(8,128)(2,1)S(1)} collective-permute-done((bf16[8,64,256]{2,1,0:T(8,128)(2,1)S(1)}, bf16[8,64,256]{2,1,0:T(8,128)(2,1)S(1)}, u32[]{:S(2)}, u32[]{:S(2)}) %collective-permute-start.13) | collective-permute-done | bytes 262176 | tf_op jit(solution)/shard_map/ppermute | solution.py:26
  138.7 4.7 %collective-permute-done.14.refs_3_ = bf16[8,64,256]{2,1,0:T(8,128)(2,1)S(1)} collective-permute-done((bf16[8,64,256]{2,1,0:T(8,128)(2,1)S(1)}, bf16[8,64,256]{2,1,0:T(8,128)(2,1)S(1)}, u32[]{:S(2)}, u32[]{:S(2)}) %collective-permute-start.14) | collective-permute-done | bytes 262176 | tf_op jit(solution)/shard_map/ppermute | solution.py:26
  (31 shorter events, 12.0 us)
Async XLA Ops:
  0.0 67.8 %copy-start = (f32[3,2048]{1,0:T(4,128)S(1)}, f32[3,2048]{1,0:T(4,128)}, u32[]{:S(2)}) copy-start(f32[3,2048]{1,0:T(4,128)} %param.12) | copy-start | bytes 73732
  19.2 32.4 %collective-permute-start = (bf16[4,64,768]{2,1,0:T(8,128)(2,1)S(1)}, bf16[4,64,768]{2,1,0:T(8,128)(2,1)S(1)}, u32[]{:S(2)}, u32[]{:S(2)}) collective-permute-start(bf16[4,64,768]{2,1,0:T(8,128)(2,1)S(1)} %all_to_all.10.refs_0_), channel_id=1, source_target_pairs={{0,992},{32,960},{64,160},{96,128},{128,96},{160,64},{192,288},{22... | collective-permute-start | bytes 1179656 | tf_op jit(solution)/shard_map/ppermute | solution.py:31
  35.2 22.2 %collective-permute-start.4 = (bf16[4,64,768]{2,1,0:T(8,128)(2,1)S(1)}, bf16[4,64,768]{2,1,0:T(8,128)(2,1)S(1)}, u32[]{:S(2)}, u32[]{:S(2)}) collective-permute-start(bf16[4,64,768]{2,1,0:T(8,128)(2,1)S(1)} %all_to_all.10.refs_0_), channel_id=1, source_target_pairs={{0,8},{8,16},{16,24},{24,0},{1,9},{9,17},{17,25},{25,1},{2,10},{10... | collective-permute-start | bytes 1179656 | tf_op jit(solution)/shard_map/ppermute | solution.py:26
  38.7 29.1 %collective-permute-start.5 = (bf16[4,64,768]{2,1,0:T(8,128)(2,1)S(1)}, bf16[4,64,768]{2,1,0:T(8,128)(2,1)S(1)}, u32[]{:S(2)}, u32[]{:S(2)}) collective-permute-start(bf16[4,64,768]{2,1,0:T(8,128)(2,1)S(1)} %all_to_all.10.refs_0_), channel_id=1, source_target_pairs={{0,24},{8,0},{16,8},{24,16},{1,25},{9,1},{17,9},{25,17},{2,26},{10... | collective-permute-start | bytes 1179656 | tf_op jit(solution)/shard_map/ppermute | solution.py:26
  41.0 26.7 %collective-permute-start.6 = (bf16[4,64,768]{2,1,0:T(8,128)(2,1)S(1)}, bf16[4,64,768]{2,1,0:T(8,128)(2,1)S(1)}, u32[]{:S(2)}, u32[]{:S(2)}) collective-permute-start(bf16[4,64,768]{2,1,0:T(8,128)(2,1)S(1)} %all_to_all.10.refs_0_), channel_id=1, source_target_pairs={{0,16},{8,24},{16,0},{24,8},{1,17},{9,25},{17,1},{25,9},{2,18},{10... | collective-permute-start | bytes 1179656 | tf_op jit(solution)/shard_map/ppermute | solution.py:26
  51.6 18.3 %collective-permute-start.1 = (bf16[4,64,768]{2,1,0:T(8,128)(2,1)S(1)}, bf16[4,64,768]{2,1,0:T(8,128)(2,1)S(1)}, u32[]{:S(2)}, u32[]{:S(2)}) collective-permute-start(bf16[4,64,768]{2,1,0:T(8,128)(2,1)S(1)} %collective-permute-done.refs_0_), channel_id=1, source_target_pairs={{0,8},{8,16},{16,24},{24,0},{1,9},{9,17},{17,25},{25,1},{2,10},{10... | collective-permute-start | bytes 1179656 | tf_op jit(solution)/shard_map/ppermute | solution.py:26
  55.0 14.8 %collective-permute-start.2 = (bf16[4,64,768]{2,1,0:T(8,128)(2,1)S(1)}, bf16[4,64,768]{2,1,0:T(8,128)(2,1)S(1)}, u32[]{:S(2)}, u32[]{:S(2)}) collective-permute-start(bf16[4,64,768]{2,1,0:T(8,128)(2,1)S(1)} %collective-permute-done.refs_0_), channel_id=1, source_target_pairs={{0,24},{8,0},{16,8},{24,16},{1,25},{9,1},{17,9},{25,17},{2,26},{10... | collective-permute-start | bytes 1179656 | tf_op jit(solution)/shard_map/ppermute | solution.py:26
  57.4 19.4 %collective-permute-start.3 = (bf16[4,64,768]{2,1,0:T(8,128)(2,1)S(1)}, bf16[4,64,768]{2,1,0:T(8,128)(2,1)S(1)}, u32[]{:S(2)}, u32[]{:S(2)}) collective-permute-start(bf16[4,64,768]{2,1,0:T(8,128)(2,1)S(1)} %collective-permute-done.refs_0_), channel_id=1, source_target_pairs={{0,16},{8,24},{16,0},{24,8},{1,17},{9,25},{17,1},{25,9},{2,18},{10... | collective-permute-start | bytes 1179656 | tf_op jit(solution)/shard_map/ppermute | solution.py:26
  61.7 1.9 %copy-start.1 = (bf16[1,768,2048]{2,1,0:T(8,128)(2,1)S(1)}, bf16[1,768,2048]{2,1,0:T(8,128)(2,1)}, u32[]{:S(2)}) copy-start(bf16[1,768,2048]{2,1,0:T(8,128)(2,1)} %param.7) | copy-start | bytes 9437188
  63.6 0.7 copy-start.2
  79.2 25.8 %copy-start.3 = (bf16[64,256]{1,0:T(8,128)(2,1)S(1)}, bf16[64,256]{1,0:T(8,128)(2,1)}, u32[]{:S(2)}) copy-start(bf16[64,256]{1,0:T(8,128)(2,1)} %param.13) | copy-start | bytes 98308
  103.1 41.5 %collective-permute-start.7 = (bf16[4,768,256]{2,1,0:T(8,128)(2,1)S(1)}, bf16[4,768,256]{2,1,0:T(8,128)(2,1)S(1)}, u32[]{:S(2)}, u32[]{:S(2)}) collective-permute-start(bf16[4,768,256]{2,1,0:T(8,128)(2,1)S(1)} %all_to_all.11.gated_ref), channel_id=1, source_target_pairs={{0,1},{1,0},{2,3},{3,2},{4,5},{5,4},{6,7},{7,6},{8,9},{9,8},{10,11... | collective-permute-start | bytes 4718600 | tf_op jit(solution)/shard_map/ppermute | solution.py:233
  105.0 7.2 %collective-permute-start.8 = (bf16[64,256]{1,0:T(8,128)(2,1)S(1)}, bf16[64,256]{1,0:T(8,128)(2,1)S(1)}, u32[]{:S(2)}, u32[]{:S(2)}) collective-permute-start(bf16[64,256]{1,0:T(8,128)(2,1)S(1)} %copy-done.3), channel_id=1, source_target_pairs={{0,32},{32,64},{64,96},{96,128},{128,160},{160,192},{192,224},{224... | collective-permute-start | bytes 98312 | tf_op jit(solution)/shard_map/ppermute | solution.py:26
  107.0 6.7 %collective-permute-start.9 = (bf16[64,256]{1,0:T(8,128)(2,1)S(1)}, bf16[64,256]{1,0:T(8,128)(2,1)S(1)}, u32[]{:S(2)}, u32[]{:S(2)}) collective-permute-start(bf16[64,256]{1,0:T(8,128)(2,1)S(1)} %copy-done.3), channel_id=1, source_target_pairs={{0,992},{32,0},{64,32},{96,64},{128,96},{160,128},{192,160},{224,1... | collective-permute-start | bytes 98312 | tf_op jit(solution)/shard_map/ppermute | solution.py:26
  113.7 10.6 %collective-permute-start.10 = (bf16[3,64,256]{2,1,0:T(8,128)(2,1)S(1)}, bf16[3,64,256]{2,1,0:T(8,128)(2,1)S(1)}, u32[]{:S(2)}, u32[]{:S(2)}) collective-permute-start(bf16[3,64,256]{2,1,0:T(8,128)(2,1)S(1)} %pad_maximum_fusion), channel_id=1, source_target_pairs={{0,96},{32,128},{64,160},{96,192},{128,224},{160,256},{192,288},{2... | collective-permute-start | bytes 294920 | tf_op jit(solution)/shard_map/ppermute | solution.py:26
  115.7 10.6 %collective-permute-start.11 = (bf16[2,64,256]{2,1,0:T(8,128)(2,1)S(1)}, bf16[2,64,256]{2,1,0:T(8,128)(2,1)S(1)}, u32[]{:S(2)}, u32[]{:S(2)}) collective-permute-start(bf16[2,64,256]{2,1,0:T(8,128)(2,1)S(1)} %pad_maximum_fusion.1), channel_id=1, source_target_pairs={{0,928},{32,960},{64,992},{96,0},{128,32},{160,64},{192,96},{224,1... | collective-permute-start | bytes 196616 | tf_op jit(solution)/shard_map/ppermute | solution.py:26
  126.3 9.1 %collective-permute-start.12 = (bf16[8,64,256]{2,1,0:T(8,128)(2,1)S(1)}, bf16[8,64,256]{2,1,0:T(8,128)(2,1)S(1)}, u32[]{:S(2)}, u32[]{:S(2)}) collective-permute-start(bf16[8,64,256]{2,1,0:T(8,128)(2,1)S(1)} %constant_dynamic-update-slice_fusion.refs_0_), channel_id=1, source_target_pairs={{0,8},{8,16},{16,24},{24,0},{1,9},{9,17},{17,25},{25,1},{2,10},{10... | collective-permute-start | bytes 786440 | tf_op jit(solution)/shard_map/ppermute | solution.py:26
  128.2 10.5 %collective-permute-start.13 = (bf16[8,64,256]{2,1,0:T(8,128)(2,1)S(1)}, bf16[8,64,256]{2,1,0:T(8,128)(2,1)S(1)}, u32[]{:S(2)}, u32[]{:S(2)}) collective-permute-start(bf16[8,64,256]{2,1,0:T(8,128)(2,1)S(1)} %constant_dynamic-update-slice_fusion.refs_0_), channel_id=1, source_target_pairs={{0,24},{8,0},{16,8},{24,16},{1,25},{9,1},{17,9},{25,17},{2,26},{10... | collective-permute-start | bytes 786440 | tf_op jit(solution)/shard_map/ppermute | solution.py:26
  132.1 11.2 %collective-permute-start.14 = (bf16[8,64,256]{2,1,0:T(8,128)(2,1)S(1)}, bf16[8,64,256]{2,1,0:T(8,128)(2,1)S(1)}, u32[]{:S(2)}, u32[]{:S(2)}) collective-permute-start(bf16[8,64,256]{2,1,0:T(8,128)(2,1)S(1)} %constant_dynamic-update-slice_fusion.refs_0_), channel_id=1, source_target_pairs={{0,16},{8,24},{16,0},{24,8},{1,17},{9,25},{17,1},{25,9},{2,18},{10... | collective-permute-start | bytes 786440 | tf_op jit(solution)/shard_map/ppermute | solution.py:26

commit v4 on v3

--- a/solution.py
+++ b/solution.py
@@ -49,29 +49,18 @@
             out_ref[p, :, k * columns : (k + 1) * columns] = held[k]
 
 
-def norm_kernel(x_ref, gain_ref, out_ref, held, sems):
-    rows = held.shape[1]
-    chunks = x_ref.shape[0] // rows
+def norm_kernel(x_ref, gain_ref, out_ref):
+    rows = 64
     gain = gain_ref[...]
-    small = 32
-
-    def fetch(i):
-        return pltpu.make_async_copy(x_ref.at[pl.ds(i * rows, rows)], held.at[i % 2], sems.at[i % 2])
-
-    fetch(0).start()
-    for i in range(chunks):
-        if i + 1 < chunks:
-            fetch(i + 1).start()
-        fetch(i).wait()
-
-        def step(j, _, i=i):
-            at = pl.multiple_of(j * small, small)
-            x = held[i % 2, pl.ds(at, small), :].astype(jnp.float32)
-            scale = lax.rsqrt(jnp.mean(x * x, axis=-1, keepdims=True) + 1e-06)
-            out_ref[pl.ds(i * rows + at, small), :] = (x * scale * gain).astype(jnp.bfloat16)
-            return 0
-
-        lax.fori_loop(0, rows // small, step, 0)
+
+    def step(i, _):
+        at = pl.ds(pl.multiple_of(i * rows, rows), rows)
+        x = x_ref[at, :].astype(jnp.float32)
+        scale = lax.rsqrt(jnp.mean(x * x, axis=-1, keepdims=True) + 1e-06)
+        out_ref[at, :] = (x * scale * gain).astype(jnp.bfloat16)
+        return 0
+
+    lax.fori_loop(0, x_ref.shape[0] // rows, step, 0)
 
 
 ROWS = 256
@@ -141,7 +130,6 @@
 
 
 VMEM = pl.BlockSpec(memory_space=pltpu.VMEM)
-HBM = pl.BlockSpec(memory_space=pltpu.HBM)
 ANY = pl.BlockSpec(memory_space=pl.ANY)
 SMEM = pl.BlockSpec(memory_space=pltpu.SMEM)
 
@@ -198,16 +186,7 @@
     other_group = mirror(group)
     near = pieces_of(group, "y")
 
-    norm = call(
-        norm_kernel,
-        (seq, width),
-        bf16,
-        [HBM, VMEM],
-        8 * seq * width,
-        4 * seq * width,
-        [pltpu.VMEM((2, 192, width), bf16), pltpu.SemaphoreType.DMA((2,))],
-        limit=9,
-    )
+    norm = call(norm_kernel, (seq, width), bf16, [VMEM] * 2, 8 * seq * width, 4 * seq * width, limit=9)
     normed = norm(tokens.reshape(seq, width), norm_gain.reshape(1, width))
     flops = 3 * seq * width * columns
     weight = pltpu.VMEM((width // 2, 3 * columns), bf16)

time: 147 us -> 147 us (level)
  Pallas kernels: 12 us -> 10.5 us
  waiting for transfers between devices: 26.5 us -> 28 us
  transfers between devices with their start and end apart: 15 -> 15, of which waited for: 8 -> 9; matrix products, arithmetic and copies ran while one was open for 0% -> 0% of each run, Pallas kernels for 5% -> 4%
where the time goes in v4:
time: 147 us; the launch traced here: 146 us
  starting transfers between devices  63 us (43%)
  blocking collectives  41.4 us (28%)
  waiting for transfers between devices  28 us (19%)
  Pallas kernels  10.5 us (7%)
  local copies, waits for them, and re-layouts  2.72 us (2%)
    ppermute x13, starting transfers between devices, shift(): return lax.ppermute(x, axis, ring(size_of(axis), step))  45 us
    all_to_all x2, blocking collectives, exchange(): return lax.all_to_all(copies, axis, 0, 0, tiled=True)  41.4 us
    ppermute x13, waiting for transfers between devices, shift(): return lax.ppermute(x, axis, ring(size_of(axis), step))  21.7 us
    ppermute x1, starting transfers between devices, mirror(): lax.ppermute(x, LINE, [(i, (i + (-1, -3, 3, 1)[i % 4]) % size) for i in r...  16 us
    ppermute x1, waiting for transfers between devices, mirror(): lax.ppermute(x, LINE, [(i, (i + (-1, -3, 3, 1)[i % 4]) % size) for i in r...  6.3 us
  transfers between devices with their start and end apart: 15, of which 9 were waited for; matrix products, arithmetic and copies ran while one was open for 0% of the time, Pallas kernels for 4%

profile of v4, /device:TPU:8, one launch (start us, length us, event | category | flops | bytes accessed | tf_op | source)
XLA Modules:
  0.0 145.9 jit_solution(6275848047286294121)
XLA Ops:
  1.6 17.6 %all_to_all.10.refs_0_ = bf16[4,64,768]{2,1,0:T(8,128)(2,1)S(1)} all-to-all(bf16[4,64,768]{2,1,0:T(8,128)(2,1)} %shard_map.74), channel_id=1, replica_groups=mesh['rep'=4,'zh'=2,'zl'=4,'y'=4,'x'=4,'core'=2] {'zl'}, dimensions={0} | all-to-all | bytes 786432 | tf_op jit(solution)/shard_map/all_to_all | solution.py:35
  19.2 16.0 %collective-permute-start = (bf16[4,64,768]{2,1,0:T(8,128)(2,1)S(1)}, bf16[4,64,768]{2,1,0:T(8,128)(2,1)S(1)}, u32[]{:S(2)}, u32[]{:S(2)}) collective-permute-start(bf16[4,64,768]{2,1,0:T(8,128)(2,1)S(1)} %all_to_all.10.refs_0_), channel_id=1, source_target_pairs={{0,992},{32,960},{64,160},{96,128},{128,96},{160,64},{192,288},{22... | collective-permute-start | bytes 1179656 | tf_op jit(solution)/shard_map/ppermute | solution.py:31
  35.2 3.5 %collective-permute-start.4 = (bf16[4,64,768]{2,1,0:T(8,128)(2,1)S(1)}, bf16[4,64,768]{2,1,0:T(8,128)(2,1)S(1)}, u32[]{:S(2)}, u32[]{:S(2)}) collective-permute-start(bf16[4,64,768]{2,1,0:T(8,128)(2,1)S(1)} %all_to_all.10.refs_0_), channel_id=1, source_target_pairs={{0,8},{8,16},{16,24},{24,0},{1,9},{9,17},{17,25},{25,1},{2,10},{10... | collective-permute-start | bytes 1179656 | tf_op jit(solution)/shard_map/ppermute | solution.py:26
  38.7 2.4 %collective-permute-start.5 = (bf16[4,64,768]{2,1,0:T(8,128)(2,1)S(1)}, bf16[4,64,768]{2,1,0:T(8,128)(2,1)S(1)}, u32[]{:S(2)}, u32[]{:S(2)}) collective-permute-start(bf16[4,64,768]{2,1,0:T(8,128)(2,1)S(1)} %all_to_all.10.refs_0_), channel_id=1, source_target_pairs={{0,24},{8,0},{16,8},{24,16},{1,25},{9,1},{17,9},{25,17},{2,26},{10... | collective-permute-start | bytes 1179656 | tf_op jit(solution)/shard_map/ppermute | solution.py:26
  41.0 4.2 %collective-permute-start.6 = (bf16[4,64,768]{2,1,0:T(8,128)(2,1)S(1)}, bf16[4,64,768]{2,1,0:T(8,128)(2,1)S(1)}, u32[]{:S(2)}, u32[]{:S(2)}) collective-permute-start(bf16[4,64,768]{2,1,0:T(8,128)(2,1)S(1)} %all_to_all.10.refs_0_), channel_id=1, source_target_pairs={{0,16},{8,24},{16,0},{24,8},{1,17},{9,25},{17,1},{25,9},{2,18},{10... | collective-permute-start | bytes 1179656 | tf_op jit(solution)/shard_map/ppermute | solution.py:26
  45.3 6.3 %collective-permute-done.refs_0_ = bf16[4,64,768]{2,1,0:T(8,128)(2,1)S(1)} collective-permute-done((bf16[4,64,768]{2,1,0:T(8,128)(2,1)S(1)}, bf16[4,64,768]{2,1,0:T(8,128)(2,1)S(1)}, u32[]{:S(2)}, u32[]{:S(2)}) %collective-permute-start) | collective-permute-done | bytes 393248 | tf_op jit(solution)/shard_map/ppermute | solution.py:31
  51.6 3.5 %collective-permute-start.1 = (bf16[4,64,768]{2,1,0:T(8,128)(2,1)S(1)}, bf16[4,64,768]{2,1,0:T(8,128)(2,1)S(1)}, u32[]{:S(2)}, u32[]{:S(2)}) collective-permute-start(bf16[4,64,768]{2,1,0:T(8,128)(2,1)S(1)} %collective-permute-done.refs_0_), channel_id=1, source_target_pairs={{0,8},{8,16},{16,24},{24,0},{1,9},{9,17},{17,25},{25,1},{2,10},{10... | collective-permute-start | bytes 1179656 | tf_op jit(solution)/shard_map/ppermute | solution.py:26
  55.0 2.4 %collective-permute-start.2 = (bf16[4,64,768]{2,1,0:T(8,128)(2,1)S(1)}, bf16[4,64,768]{2,1,0:T(8,128)(2,1)S(1)}, u32[]{:S(2)}, u32[]{:S(2)}) collective-permute-start(bf16[4,64,768]{2,1,0:T(8,128)(2,1)S(1)} %collective-permute-done.refs_0_), channel_id=1, source_target_pairs={{0,24},{8,0},{16,8},{24,16},{1,25},{9,1},{17,9},{25,17},{2,26},{10... | collective-permute-start | bytes 1179656 | tf_op jit(solution)/shard_map/ppermute | solution.py:26
  57.4 4.2 %collective-permute-start.3 = (bf16[4,64,768]{2,1,0:T(8,128)(2,1)S(1)}, bf16[4,64,768]{2,1,0:T(8,128)(2,1)S(1)}, u32[]{:S(2)}, u32[]{:S(2)}) collective-permute-start(bf16[4,64,768]{2,1,0:T(8,128)(2,1)S(1)} %collective-permute-done.refs_0_), channel_id=1, source_target_pairs={{0,16},{8,24},{16,0},{24,8},{1,17},{9,25},{17,1},{25,9},{2,18},{10... | collective-permute-start | bytes 1179656 | tf_op jit(solution)/shard_map/ppermute | solution.py:26
  64.3 2.0 %shard_map.73.normed_ref = bf16[768,2048]{1,0:T(8,128)(2,1)S(1)} custom-call(bf16[768,2048]{1,0:T(8,128)(2,1)S(1)} %bitcast.14, f32[1,2048]{1,0:T(1,128)S(1)} %bitcast.15), custom_call_target="tpu_custom_call" | custom-call | flops 12582912 | bytes 6291456 | tf_op jit(solution)/shard_map/pallas_call | solution.py:190
  66.3 2.0 %shard_map.75.refs_4_ = f32[768,768]{1,0:T(8,128)S(1)} custom-call(s32[5]{0:T(128)S(1)} %stack.37.at_ref, bf16[768,2048]{1,0:T(8,128)(2,1)S(1)} %shard_map.73.normed_ref, bf16[4,64,768]{2,1,0:T(8,128)(2,1)S(1)} %all_to_all.10.refs_0_, bf16[4,64,768]{2,1,0:T(8,128)(2,1)S(1)} %collective-permute-done.4.refs_1_, ...), custom_call_target="tpu_custom_call" | custom-call | flops 1207959552 | bytes 12582912 | tf_op jit(solution)/shard_map/pallas_call | solution.py:194
  68.8 8.0 %collective-permute-done.3.refs_3_ = bf16[4,64,768]{2,1,0:T(8,128)(2,1)S(1)} collective-permute-done((bf16[4,64,768]{2,1,0:T(8,128)(2,1)S(1)}, bf16[4,64,768]{2,1,0:T(8,128)(2,1)S(1)}, u32[]{:S(2)}, u32[]{:S(2)}) %collective-permute-start.3) | collective-permute-done | bytes 393248 | tf_op jit(solution)/shard_map/ppermute | solution.py:26
  76.8 2.4 %shard_map.76 = bf16[4,768,256]{2,1,0:T(8,128)(2,1)S(1)} custom-call(s32[5]{0:T(128)S(1)} %stack.37.at_ref, bf16[768,2048]{1,0:T(8,128)(2,1)S(1)} %shard_map.73.normed_ref, bf16[4,64,768]{2,1,0:T(8,128)(2,1)S(1)} %collective-permute-done.refs_0_, bf16[4,64,768]{2,1,0:T(8,128)(2,1)S(1)} %collective-permute-done.1.refs_1_, ...), custom_call_target="tpu_custom_call" | custom-call | flops 1207959552 | bytes 12582912 | tf_op jit(solution)/shard_map/pallas_call | solution.py:209
  79.3 23.9 %all_to_all.11.gated_ref = bf16[4,768,256]{2,1,0:T(8,128)(2,1)S(1)} all-to-all(bf16[4,768,256]{2,1,0:T(8,128)(2,1)S(1)} %shard_map.76), channel_id=1, replica_groups=mesh['rep'=4,'zh'=2,'zl'=4,'y'=4,'x'=4,'core'=2] {'x'}, dimensions={0} | all-to-all | bytes 3145728 | tf_op jit(solution)/shard_map/all_to_all | solution.py:35
  103.1 1.9 %collective-permute-start.7 = (bf16[4,768,256]{2,1,0:T(8,128)(2,1)S(1)}, bf16[4,768,256]{2,1,0:T(8,128)(2,1)S(1)}, u32[]{:S(2)}, u32[]{:S(2)}) collective-permute-start(bf16[4,768,256]{2,1,0:T(8,128)(2,1)S(1)} %all_to_all.11.gated_ref), channel_id=1, source_target_pairs={{0,1},{1,0},{2,3},{3,2},{4,5},{5,4},{6,7},{7,6},{8,9},{9,8},{10,11... | collective-permute-start | bytes 4718600 | tf_op jit(solution)/shard_map/ppermute | solution.py:212
  105.0 1.9 %collective-permute-start.8 = (bf16[64,256]{1,0:T(8,128)(2,1)S(1)}, bf16[64,256]{1,0:T(8,128)(2,1)S(1)}, u32[]{:S(2)}, u32[]{:S(2)}) collective-permute-start(bf16[64,256]{1,0:T(8,128)(2,1)S(1)} %copy-done.3), channel_id=1, source_target_pairs={{0,32},{32,64},{64,96},{96,128},{128,160},{160,192},{192,224},{224... | collective-permute-start | bytes 98312 | tf_op jit(solution)/shard_map/ppermute | solution.py:26
  107.0 5.2 %collective-permute-start.9 = (bf16[64,256]{1,0:T(8,128)(2,1)S(1)}, bf16[64,256]{1,0:T(8,128)(2,1)S(1)}, u32[]{:S(2)}, u32[]{:S(2)}) collective-permute-start(bf16[64,256]{1,0:T(8,128)(2,1)S(1)} %copy-done.3), channel_id=1, source_target_pairs={{0,992},{32,0},{64,32},{96,64},{128,96},{160,128},{192,160},{224,1... | collective-permute-start | bytes 98312 | tf_op jit(solution)/shard_map/ppermute | solution.py:26
  113.7 1.9 %collective-permute-start.10 = (bf16[3,64,256]{2,1,0:T(8,128)(2,1)S(1)}, bf16[3,64,256]{2,1,0:T(8,128)(2,1)S(1)}, u32[]{:S(2)}, u32[]{:S(2)}) collective-permute-start(bf16[3,64,256]{2,1,0:T(8,128)(2,1)S(1)} %pad_maximum_fusion), channel_id=1, source_target_pairs={{0,96},{32,128},{64,160},{96,192},{128,224},{160,256},{192,288},{2... | collective-permute-start | bytes 294920 | tf_op jit(solution)/shard_map/ppermute | solution.py:26
  115.7 6.9 %collective-permute-start.11 = (bf16[2,64,256]{2,1,0:T(8,128)(2,1)S(1)}, bf16[2,64,256]{2,1,0:T(8,128)(2,1)S(1)}, u32[]{:S(2)}, u32[]{:S(2)}) collective-permute-start(bf16[2,64,256]{2,1,0:T(8,128)(2,1)S(1)} %pad_maximum_fusion.1), channel_id=1, source_target_pairs={{0,928},{32,960},{64,992},{96,0},{128,32},{160,64},{192,96},{224,1... | collective-permute-start | bytes 196616 | tf_op jit(solution)/shard_map/ppermute | solution.py:26
  124.4 1.9 %collective-permute-done.11 = bf16[2,64,256]{2,1,0:T(8,128)(2,1)S(1)} collective-permute-done((bf16[2,64,256]{2,1,0:T(8,128)(2,1)S(1)}, bf16[2,64,256]{2,1,0:T(8,128)(2,1)S(1)}, u32[]{:S(2)}, u32[]{:S(2)}) %collective-permute-start.11) | collective-permute-done | bytes 65568 | tf_op jit(solution)/shard_map/ppermute | solution.py:26
  128.2 3.9 %collective-permute-start.13 = (bf16[8,64,256]{2,1,0:T(8,128)(2,1)S(1)}, bf16[8,64,256]{2,1,0:T(8,128)(2,1)S(1)}, u32[]{:S(2)}, u32[]{:S(2)}) collective-permute-start(bf16[8,64,256]{2,1,0:T(8,128)(2,1)S(1)} %constant_dynamic-update-slice_fusion.refs_0_), channel_id=1, source_target_pairs={{0,24},{8,0},{16,8},{24,16},{1,25},{9,1},{17,9},{25,17},{2,26},{10... | collective-permute-start | bytes 786440 | tf_op jit(solution)/shard_map/ppermute | solution.py:26
  132.1 3.2 %collective-permute-start.14 = (bf16[8,64,256]{2,1,0:T(8,128)(2,1)S(1)}, bf16[8,64,256]{2,1,0:T(8,128)(2,1)S(1)}, u32[]{:S(2)}, u32[]{:S(2)}) collective-permute-start(bf16[8,64,256]{2,1,0:T(8,128)(2,1)S(1)} %constant_dynamic-update-slice_fusion.refs_0_), channel_id=1, source_target_pairs={{0,16},{8,24},{16,0},{24,8},{1,17},{9,25},{17,1},{25,9},{2,18},{10... | collective-permute-start | bytes 786440 | tf_op jit(solution)/shard_map/ppermute | solution.py:26
  135.4 3.3 %collective-permute-done.13.refs_2_ = bf16[8,64,256]{2,1,0:T(8,128)(2,1)S(1)} collective-permute-done((bf16[8,64,256]{2,1,0:T(8,128)(2,1)S(1)}, bf16[8,64,256]{2,1,0:T(8,128)(2,1)S(1)}, u32[]{:S(2)}, u32[]{:S(2)}) %collective-permute-start.13) | collective-permute-done | bytes 262176 | tf_op jit(solution)/shard_map/ppermute | solution.py:26
  138.7 4.7 %collective-permute-done.14.refs_3_ = bf16[8,64,256]{2,1,0:T(8,128)(2,1)S(1)} collective-permute-done((bf16[8,64,256]{2,1,0:T(8,128)(2,1)S(1)}, bf16[8,64,256]{2,1,0:T(8,128)(2,1)S(1)}, u32[]{:S(2)}, u32[]{:S(2)}) %collective-permute-start.14) | collective-permute-done | bytes 262176 | tf_op jit(solution)/shard_map/ppermute | solution.py:26
  (31 shorter events, 12.4 us)
Async XLA Ops:
  0.0 66.3 %copy-start = (f32[3,2048]{1,0:T(4,128)S(1)}, f32[3,2048]{1,0:T(4,128)}, u32[]{:S(2)}) copy-start(f32[3,2048]{1,0:T(4,128)} %param.12) | copy-start | bytes 73732
  19.2 32.4 %collective-permute-start = (bf16[4,64,768]{2,1,0:T(8,128)(2,1)S(1)}, bf16[4,64,768]{2,1,0:T(8,128)(2,1)S(1)}, u32[]{:S(2)}, u32[]{:S(2)}) collective-permute-start(bf16[4,64,768]{2,1,0:T(8,128)(2,1)S(1)} %all_to_all.10.refs_0_), channel_id=1, source_target_pairs={{0,992},{32,960},{64,160},{96,128},{128,96},{160,64},{192,288},{22... | collective-permute-start | bytes 1179656 | tf_op jit(solution)/shard_map/ppermute | solution.py:31
  35.2 22.2 %collective-permute-start.4 = (bf16[4,64,768]{2,1,0:T(8,128)(2,1)S(1)}, bf16[4,64,768]{2,1,0:T(8,128)(2,1)S(1)}, u32[]{:S(2)}, u32[]{:S(2)}) collective-permute-start(bf16[4,64,768]{2,1,0:T(8,128)(2,1)S(1)} %all_to_all.10.refs_0_), channel_id=1, source_target_pairs={{0,8},{8,16},{16,24},{24,0},{1,9},{9,17},{17,25},{25,1},{2,10},{10... | collective-permute-start | bytes 1179656 | tf_op jit(solution)/shard_map/ppermute | solution.py:26
  38.7 27.6 %collective-permute-start.5 = (bf16[4,64,768]{2,1,0:T(8,128)(2,1)S(1)}, bf16[4,64,768]{2,1,0:T(8,128)(2,1)S(1)}, u32[]{:S(2)}, u32[]{:S(2)}) collective-permute-start(bf16[4,64,768]{2,1,0:T(8,128)(2,1)S(1)} %all_to_all.10.refs_0_), channel_id=1, source_target_pairs={{0,24},{8,0},{16,8},{24,16},{1,25},{9,1},{17,9},{25,17},{2,26},{10... | collective-permute-start | bytes 1179656 | tf_op jit(solution)/shard_map/ppermute | solution.py:26
  41.0 25.3 %collective-permute-start.6 = (bf16[4,64,768]{2,1,0:T(8,128)(2,1)S(1)}, bf16[4,64,768]{2,1,0:T(8,128)(2,1)S(1)}, u32[]{:S(2)}, u32[]{:S(2)}) collective-permute-start(bf16[4,64,768]{2,1,0:T(8,128)(2,1)S(1)} %all_to_all.10.refs_0_), channel_id=1, source_target_pairs={{0,16},{8,24},{16,0},{24,8},{1,17},{9,25},{17,1},{25,9},{2,18},{10... | collective-permute-start | bytes 1179656 | tf_op jit(solution)/shard_map/ppermute | solution.py:26
  51.6 16.8 %collective-permute-start.1 = (bf16[4,64,768]{2,1,0:T(8,128)(2,1)S(1)}, bf16[4,64,768]{2,1,0:T(8,128)(2,1)S(1)}, u32[]{:S(2)}, u32[]{:S(2)}) collective-permute-start(bf16[4,64,768]{2,1,0:T(8,128)(2,1)S(1)} %collective-permute-done.refs_0_), channel_id=1, source_target_pairs={{0,8},{8,16},{16,24},{24,0},{1,9},{9,17},{17,25},{25,1},{2,10},{10... | collective-permute-start | bytes 1179656 | tf_op jit(solution)/shard_map/ppermute | solution.py:26
  55.0 13.8 %collective-permute-start.2 = (bf16[4,64,768]{2,1,0:T(8,128)(2,1)S(1)}, bf16[4,64,768]{2,1,0:T(8,128)(2,1)S(1)}, u32[]{:S(2)}, u32[]{:S(2)}) collective-permute-start(bf16[4,64,768]{2,1,0:T(8,128)(2,1)S(1)} %collective-permute-done.refs_0_), channel_id=1, source_target_pairs={{0,24},{8,0},{16,8},{24,16},{1,25},{9,1},{17,9},{25,17},{2,26},{10... | collective-permute-start | bytes 1179656 | tf_op jit(solution)/shard_map/ppermute | solution.py:26
  57.4 19.4 %collective-permute-start.3 = (bf16[4,64,768]{2,1,0:T(8,128)(2,1)S(1)}, bf16[4,64,768]{2,1,0:T(8,128)(2,1)S(1)}, u32[]{:S(2)}, u32[]{:S(2)}) collective-permute-start(bf16[4,64,768]{2,1,0:T(8,128)(2,1)S(1)} %collective-permute-done.refs_0_), channel_id=1, source_target_pairs={{0,16},{8,24},{16,0},{24,8},{1,17},{9,25},{17,1},{25,9},{2,18},{10... | collective-permute-start | bytes 1179656 | tf_op jit(solution)/shard_map/ppermute | solution.py:26
  61.7 1.9 %copy-start.1 = (bf16[1,768,2048]{2,1,0:T(8,128)(2,1)S(1)}, bf16[1,768,2048]{2,1,0:T(8,128)(2,1)}, u32[]{:S(2)}) copy-start(bf16[1,768,2048]{2,1,0:T(8,128)(2,1)} %param.7) | copy-start | bytes 9437188
  63.6 0.7 copy-start.2
  79.2 25.8 %copy-start.3 = (bf16[64,256]{1,0:T(8,128)(2,1)S(1)}, bf16[64,256]{1,0:T(8,128)(2,1)}, u32[]{:S(2)}) copy-start(bf16[64,256]{1,0:T(8,128)(2,1)} %param.13) | copy-start | bytes 98308
  103.1 41.5 %collective-permute-start.7 = (bf16[4,768,256]{2,1,0:T(8,128)(2,1)S(1)}, bf16[4,768,256]{2,1,0:T(8,128)(2,1)S(1)}, u32[]{:S(2)}, u32[]{:S(2)}) collective-permute-start(bf16[4,768,256]{2,1,0:T(8,128)(2,1)S(1)} %all_to_all.11.gated_ref), channel_id=1, source_target_pairs={{0,1},{1,0},{2,3},{3,2},{4,5},{5,4},{6,7},{7,6},{8,9},{9,8},{10,11... | collective-permute-start | bytes 4718600 | tf_op jit(solution)/shard_map/ppermute | solution.py:212
  105.0 7.2 %collective-permute-start.8 = (bf16[64,256]{1,0:T(8,128)(2,1)S(1)}, bf16[64,256]{1,0:T(8,128)(2,1)S(1)}, u32[]{:S(2)}, u32[]{:S(2)}) collective-permute-start(bf16[64,256]{1,0:T(8,128)(2,1)S(1)} %copy-done.3), channel_id=1, source_target_pairs={{0,32},{32,64},{64,96},{96,128},{128,160},{160,192},{192,224},{224... | collective-permute-start | bytes 98312 | tf_op jit(solution)/shard_map/ppermute | solution.py:26
  107.0 6.7 %collective-permute-start.9 = (bf16[64,256]{1,0:T(8,128)(2,1)S(1)}, bf16[64,256]{1,0:T(8,128)(2,1)S(1)}, u32[]{:S(2)}, u32[]{:S(2)}) collective-permute-start(bf16[64,256]{1,0:T(8,128)(2,1)S(1)} %copy-done.3), channel_id=1, source_target_pairs={{0,992},{32,0},{64,32},{96,64},{128,96},{160,128},{192,160},{224,1... | collective-permute-start | bytes 98312 | tf_op jit(solution)/shard_map/ppermute | solution.py:26
  113.7 10.6 %collective-permute-start.10 = (bf16[3,64,256]{2,1,0:T(8,128)(2,1)S(1)}, bf16[3,64,256]{2,1,0:T(8,128)(2,1)S(1)}, u32[]{:S(2)}, u32[]{:S(2)}) collective-permute-start(bf16[3,64,256]{2,1,0:T(8,128)(2,1)S(1)} %pad_maximum_fusion), channel_id=1, source_target_pairs={{0,96},{32,128},{64,160},{96,192},{128,224},{160,256},{192,288},{2... | collective-permute-start | bytes 294920 | tf_op jit(solution)/shard_map/ppermute | solution.py:26
  115.7 10.6 %collective-permute-start.11 = (bf16[2,64,256]{2,1,0:T(8,128)(2,1)S(1)}, bf16[2,64,256]{2,1,0:T(8,128)(2,1)S(1)}, u32[]{:S(2)}, u32[]{:S(2)}) collective-permute-start(bf16[2,64,256]{2,1,0:T(8,128)(2,1)S(1)} %pad_maximum_fusion.1), channel_id=1, source_target_pairs={{0,928},{32,960},{64,992},{96,0},{128,32},{160,64},{192,96},{224,1... | collective-permute-start | bytes 196616 | tf_op jit(solution)/shard_map/ppermute | solution.py:26
  126.3 9.1 %collective-permute-start.12 = (bf16[8,64,256]{2,1,0:T(8,128)(2,1)S(1)}, bf16[8,64,256]{2,1,0:T(8,128)(2,1)S(1)}, u32[]{:S(2)}, u32[]{:S(2)}) collective-permute-start(bf16[8,64,256]{2,1,0:T(8,128)(2,1)S(1)} %constant_dynamic-update-slice_fusion.refs_0_), channel_id=1, source_target_pairs={{0,8},{8,16},{16,24},{24,0},{1,9},{9,17},{17,25},{25,1},{2,10},{10... | collective-permute-start | bytes 786440 | tf_op jit(solution)/shard_map/ppermute | solution.py:26
  128.2 10.5 %collective-permute-start.13 = (bf16[8,64,256]{2,1,0:T(8,128)(2,1)S(1)}, bf16[8,64,256]{2,1,0:T(8,128)(2,1)S(1)}, u32[]{:S(2)}, u32[]{:S(2)}) collective-permute-start(bf16[8,64,256]{2,1,0:T(8,128)(2,1)S(1)} %constant_dynamic-update-slice_fusion.refs_0_), channel_id=1, source_target_pairs={{0,24},{8,0},{16,8},{24,16},{1,25},{9,1},{17,9},{25,17},{2,26},{10... | collective-permute-start | bytes 786440 | tf_op jit(solution)/shard_map/ppermute | solution.py:26
  132.1 11.2 %collective-permute-start.14 = (bf16[8,64,256]{2,1,0:T(8,128)(2,1)S(1)}, bf16[8,64,256]{2,1,0:T(8,128)(2,1)S(1)}, u32[]{:S(2)}, u32[]{:S(2)}) collective-permute-start(bf16[8,64,256]{2,1,0:T(8,128)(2,1)S(1)} %constant_dynamic-update-slice_fusion.refs_0_), channel_id=1, source_target_pairs={{0,16},{8,24},{16,0},{24,8},{1,17},{9,25},{17,1},{25,9},{2,18},{10... | collective-permute-start | bytes 786440 | tf_op jit(solution)/shard_map/ppermute | solution.py:26
